TPU v7x, 512 devices: a whole 4x4x16 slice. The times are simulated.
512 devices in a mesh: fs: 128 (over z, x, core), tp: 4 (over y).
Axes of the slice: x: 4, y: 4, z: 16, core: 2. Of those that a mesh axis runs over, the one named last changes fastest.
Arguments:
- tokens: bfloat16 [1024, 2048], P(('fs', 'tp')), may hold values from -6 to 6
- route_experts: int32 [1024, 2], P(('fs', 'tp')), may hold values from 0 to 3, as said below
- route_logits: float32 [1024, 2], P(('fs', 'tp')), may hold values from -8 to 8
- norm_gain: float32 [2048], P('fs'), may hold values from 0.1 to 1.9
- gate_train: float32 [4, 2048, 8192], P(None, 'fs', 'tp'), may hold values from -0.125 to 0.125
- up_train: float32 [4, 2048, 8192], P(None, 'fs', 'tp'), may hold values from -0.125 to 0.125
- down_train: float32 [4, 2048, 8192], P(None, 'fs', 'tp'), may hold values from -0.125 to 0.125
Outputs:
- gate_serve: bfloat16 [128, 2048, 256], P('fs')
- up_serve: bfloat16 [128, 2048, 256], P('fs')
- down_serve: bfloat16 [128, 2048, 256], P('fs')
- mixed: bfloat16 [1024, 2048], P(('fs', 'tp'))
Inputs may be any that keep to these rules, and one draw needn't show every extreme that they name: `route_experts`: the two experts of a row differ; any expert may be named by every row of the devices that share one index along tp, and in every draw some expert is.
All inputs are finite; a program needn't handle non-finite values.
Results may differ from a plain program's by a relative error of at most 0.0085.
Values may be sent and summed in bfloat16 or wider, within the bound.
No kernel may reach another device: no remote copies, remote signals or barrier semaphores. Data moves between devices by JAX's collectives and lax.ppermute only.
A program may use at most 64 MiB of HBM per device.

v0:
```python
import jax
import jax.numpy as jnp
from jax import lax
from jax.experimental import pallas as pl
from jax.experimental.pallas import tpu as pltpu
from jax.sharding import Mesh
from jax.sharding import PartitionSpec as P


FS = ("z", "x", "c")
FS_TP = ("z", "x", "c", "y")
NZ, NX, NC, NY = 16, 4, 2, 4
XC = NX * NC
PAD = 128


def normalize(tokens):
    values = tokens.astype(jnp.float32)
    row_mean = jnp.mean(values, axis=-1, keepdims=True)
    centered = values - row_mean
    row_var = jnp.mean(centered * centered, axis=-1, keepdims=True)
    return (centered * lax.rsqrt(row_var + 1e-05)).astype(jnp.bfloat16)


def route_table(route_experts, route_logits, count):
    first = jax.nn.sigmoid(route_logits[:, 0] - route_logits[:, 1])
    second = jax.nn.sigmoid(route_logits[:, 1] - route_logits[:, 0])
    labels = jnp.arange(count, dtype=jnp.int32)
    table = first[:, None] * (route_experts[:, 0:1] == labels[None, :]).astype(jnp.float32)
    table = table + second[:, None] * (route_experts[:, 1:2] == labels[None, :]).astype(jnp.float32)
    return table.astype(jnp.bfloat16)


def shift(array, axis, by, size):
    return lax.ppermute(array, axis, [(i, (i + by) % size) for i in range(size)])


def swap_core(array):
    return lax.ppermute(array, "c", [(0, 1), (1, 0)])


def pack_kernel(x_ref, gain, gate, up, down, out):
    experts, block = gate.shape[0], out.shape[-1]
    depth = gain.shape[1]
    line = lax.broadcasted_iota(jnp.int32, (depth, depth), 0)
    lane = lax.broadcasted_iota(jnp.int32, (depth, depth), 1)
    wide = jnp.broadcast_to(gain[...], (depth, depth))
    scale = jnp.sum(jnp.where(line == lane, wide, 0.0), axis=1, keepdims=True)
    for y in range(NY):
        e = lax.rem(x_ref[0] + y, experts)
        for s in range(XC):
            cut = slice(s * block, (s + 1) * block)
            out[s, y, 0] = (scale * gate[e, :, cut]).astype(jnp.bfloat16)
            out[s, y, 1] = (scale * up[e, :, cut]).astype(jnp.bfloat16)
            out[s, y, 2] = down[e, :, cut].astype(jnp.bfloat16)


def sort_kernel(y_ref, swapped, riders, early, late):
    depth = swapped.shape[3]
    for e in range(NZ // NY):
        x = lax.rem(NX + e - y_ref[0], NX)
        for y in range(NY):
            for c in range(NC):
                part = swapped[NC * x + c, y]
                early[NY * e + y, depth * c : depth * (c + 1)] = part[0]
                early[NY * e + y, depth * (NC + c) : depth * (NC + c + 1)] = part[1]
                late[NY * e + y, depth * c : depth * (c + 1)] = part[2]
            early[NY * e + y, 2 * NC * depth :] = riders[...]


def put(first_ref, ins, outs):
    for k, part in enumerate(ins):
        at = lax.rem(first_ref[0] + k, NX)
        for m, out in enumerate(outs):
            span = out.shape[2]
            out[:, at] = part[:, m * span : (m + 1) * span]


def all_y(own):
    return [own] + [shift(own, "y", k, NY) for k in range(1, NY)]


def hidden_kernel(first_ref, expert_ref, *refs):
    parts, (here, there, gate, up, out, rows) = refs[:NY], refs[NY:]
    put(first_ref, parts, (gate, up))
    half = here.shape[0]
    rows[:half] = here[...]
    rows[half:] = there[...]
    width = gate.shape[0] * gate.shape[1] * gate.shape[2]
    table = rows[:, width:].astype(jnp.float32)
    lane = lax.broadcasted_iota(jnp.int32, table.shape, 1)
    weight = jnp.sum(jnp.where(lane == expert_ref[0], table, 0.0), axis=1, keepdims=True)
    x = rows[:, :width]
    g = jnp.dot(x, gate[...].reshape(width, -1), preferred_element_type=jnp.float32)
    u = jnp.dot(x, up[...].reshape(width, -1), preferred_element_type=jnp.float32)
    out[...] = (weight * (g / (1.0 + jnp.exp(-g))) * u).astype(jnp.bfloat16)


def down_kernel(first_ref, x_ref, *refs):
    parts, (hidden, down, theirs, mine) = refs[:NY], refs[NY:]
    put(first_ref, parts, (down,))
    full = down[...].reshape(-1, down.shape[3])
    half = hidden.shape[0] // 2
    dims = (((1,), (1,)), ((), ()))
    both = lax.dot_general(hidden[...], full, dims, preferred_element_type=jnp.float32)
    both = both.reshape(2, NX, half // NX, both.shape[1])
    for k in range(NX):
        to = lax.rem(NX + x_ref[0] - k, NX)
        mine[to] = both[0, k]
        theirs[to] = both[1, k].astype(jnp.bfloat16)


def per_device(tokens, route_experts, route_logits, norm_gain, gate_train, up_train, down_train):
    experts, depth, wide = gate_train.shape
    own_rows, width = tokens.shape
    block = wide // XC
    smem, vmem = pl.BlockSpec(memory_space=pltpu.SMEM), pl.BlockSpec(memory_space=pltpu.VMEM)
    y, x = lax.axis_index("y"), lax.axis_index("x")
    expert = lax.axis_index("z") // (NZ // experts)
    first_block = lax.rem(NX + expert - y, NX).reshape(1).astype(jnp.int32)
    expert, y, x = (i.reshape(1).astype(jnp.int32) for i in (expert, y, x))

    local = pl.pallas_call(
        pack_kernel,
        out_shape=jax.ShapeDtypeStruct((XC, NY, 3, depth, block), jnp.bfloat16),
        in_specs=[smem] + [vmem] * 4,
        out_specs=vmem,
    )(x, norm_gain[None, :], gate_train, up_train, down_train)
    swapped = lax.all_to_all(
        local.reshape(XC * NY, 3, depth, block), ("x", "c", "y"), 0, 0, tiled=True
    )

    normed = normalize(tokens)
    table = route_table(route_experts, route_logits, experts)
    spread = own_rows * width // block
    riders = jnp.concatenate(
        [
            normed.reshape(spread, block),
            jnp.pad(table, ((0, 8 - own_rows), (0, block - experts))),
        ]
    )
    span = NC * depth
    early, late = pl.pallas_call(
        sort_kernel,
        out_shape=[
            jax.ShapeDtypeStruct((NZ, 2 * span + spread + 8, block), jnp.bfloat16),
            jax.ShapeDtypeStruct((NZ, span, block), jnp.bfloat16),
        ],
        in_specs=[smem, vmem, vmem],
        out_specs=[vmem, vmem],
    )(y, swapped.reshape(XC, NY, 3, depth, block), riders)
    first = lax.all_to_all(early, "z", 0, 0, tiled=True)
    first, late = lax.optimization_barrier((first, late))
    second = lax.all_to_all(late, "z", 0, 0, tiled=True)

    cut = 2 * span
    parts = all_y(first[:, :cut])
    rows_z = first[:, cut : cut + spread].reshape(NZ * own_rows, width)
    table_z = first[:, cut + spread : cut + spread + own_rows, :PAD]
    rows_z = jnp.concatenate([rows_z, table_z.reshape(NZ * own_rows, PAD)], axis=1)
    rows_x = [rows_z] + [shift(rows_z, "x", k, NX) for k in range(1, NX)]
    rows_x = jnp.concatenate(rows_x)
    rows_c = swap_core(rows_x)
    placed = jax.ShapeDtypeStruct((NZ, NX, span, block), jnp.bfloat16)
    gate_serve, up_serve, hidden = pl.pallas_call(
        hidden_kernel,
        out_shape=[
            placed,
            placed,
            jax.ShapeDtypeStruct((2 * rows_x.shape[0], block), jnp.bfloat16),
        ],
        in_specs=[smem, smem] + [vmem] * (len(parts) + 2),
        out_specs=[vmem] * 3,
        scratch_shapes=[pltpu.VMEM((2 * rows_x.shape[0], width + PAD), jnp.bfloat16)],
    )(first_block, expert, *parts, rows_x, rows_c)

    parts = all_y(second)
    half = rows_x.shape[0]
    down_serve, theirs, mine = pl.pallas_call(
        down_kernel,
        out_shape=[
            placed,
            jax.ShapeDtypeStruct((NX, half // NX, width), jnp.bfloat16),
            jax.ShapeDtypeStruct((NX, half // NX, width), jnp.float32),
        ],
        in_specs=[smem, smem] + [vmem] * (len(parts) + 1),
        out_specs=[vmem] * 3,
    )(first_block, x, *parts, hidden)
    gate_serve, up_serve, down_serve = (
        matrix.reshape(1, width, block) for matrix in (gate_serve, up_serve, down_serve)
    )

    chip = (mine + swap_core(theirs).astype(jnp.float32)).astype(jnp.bfloat16)
    by_x = lax.all_to_all(chip, "x", 0, 0, tiled=True).astype(jnp.float32).sum(axis=0)
    by_x = by_x.astype(jnp.bfloat16).reshape(NZ, own_rows, width)
    by_z = lax.all_to_all(by_x, "z", 0, 0, tiled=True).astype(jnp.float32).sum(axis=0)
    return (gate_serve, up_serve, down_serve, by_z.astype(jnp.bfloat16))


def solution(mesh):
    finer = Mesh(mesh.devices.reshape(NZ, NX, NC, NY), FS_TP)
    in_specs = (
        P(FS_TP, None),
        P(FS_TP, None),
        P(FS_TP, None),
        P(FS),
        P(None, FS, "y"),
        P(None, FS, "y"),
        P(None, FS, "y"),
    )
    out_specs = (P(FS, None, None), P(FS, None, None), P(FS, None, None), P(FS_TP, None))
    return jax.shard_map(
        per_device, mesh=finer, in_specs=in_specs, out_specs=out_specs, check_vma=False
    )
```

profile of v0, /device:TPU:24, one launch (start us, length us, event | category | flops | bytes accessed | tf_op | source)
XLA Modules:
  0.0 184.6 jit_solution(17580053623482387362)
XLA Ops:
  0.6 2.4 %shard_map.102 = bf16[8,4,3,16,256]{4,3,2,1,0:T(8,128)(2,1)} custom-call(s32[1]{0:T(128)} %bitcast.3.x_ref, f32[1,16]{1,0:T(1,128)} %bitcast.15, f32[4,16,2048]{2,1,0:T(8,128)} %gate.1, f32[4,16,2048]{2,1,0:T(8,128)} %up.1, f32[4,16,2048]{2,1,0:T(8,128)} %down.1), custom_call_target="tpu_custom_call" | custom-call | tf_op jit(solution)/shard_map/pallas_call | solution.py:123
  3.0 0.0 copy-start.8
  3.0 0.0 copy-start.9
  3.0 9.3 %all-to-all-start = ((bf16[32,3,16,256]{3,2,1,0:T(8,128)(2,1)}), bf16[32,3,16,256]{3,2,1,0:T(8,128)(2,1)S(1)}, u32[]{:S(2)}, u32[]{:S(2)}) async-start(bf16[32,3,16,256]{3,2,1,0:T(8,128)(2,1)} %bitcast.12), calls=%async_computation | async-start | bytes 1572864 | tf_op jit(solution)/shard_map/all_to_all | solution.py:129
  12.3 0.0 copy-done.8
  12.3 0.1 convert_reduce_fusion
  12.5 0.2 fusion.3
  12.7 0.1 fusion.4
  12.8 0.0 copy-done.9
  12.8 0.2 slice_reduce_fusion.1
  13.0 0.0 copy-done.10
  13.0 0.2 fusion.8
  13.2 0.1 fusion.7
  13.3 0.6 fusion.5.riders
  13.9 11.0 %all-to-all-done = bf16[32,3,16,256]{3,2,1,0:T(8,128)(2,1)S(1)} async-done(((bf16[32,3,16,256]{3,2,1,0:T(8,128)(2,1)}), bf16[32,3,16,256]{3,2,1,0:T(8,128)(2,1)S(1)}, u32[]{:S(2)}, u32[]{:S(2)}) %all-to-all-start) | async-done | bytes 786464 | tf_op jit(solution)/shard_map/all_to_all | solution.py:129
  24.9 0.9 copy-done
  25.8 2.1 %shard_map.103 = (bf16[16,88,256]{2,1,0:T(8,128)(2,1)}, bf16[16,32,256]{2,1,0:T(8,128)(2,1)}) custom-call(s32[1]{0:T(128)} %bitcast.2.y_ref, bf16[8,4,3,16,256]{4,3,2,1,0:T(8,128)(2,1)} %bitcast.11, bf16[24,256]{1,0:T(8,128)(2,1)} %fusion.5.riders), custom_call_target="tpu_custom_call" | custom-call | tf_op jit(solution)/shard_map/pallas_call | solution.py:143
  27.9 51.9 %all_to_all.25 = bf16[16,88,256]{2,1,0:T(8,128)(2,1)S(1)} all-to-all(bf16[16,88,256]{2,1,0:T(8,128)(2,1)} %get-tuple-element.14), channel_id=1, replica_groups=mesh['z'=16,'x'=4,'c'=2,'y'=4] {'z'}, dimensions={0} | all-to-all | bytes 1441792 | tf_op jit(solution)/shard_map/all_to_all | solution.py:152
  79.9 0.1 reshape.66
  80.0 5.2 %all-to-all-start.2 = ((bf16[16,32,256]{2,1,0:T(8,128)(2,1)}), bf16[16,32,256]{2,1,0:T(8,128)(2,1)S(1)}, u32[]{:S(2)}, u32[]{:S(2)}) async-start(bf16[16,32,256]{2,1,0:T(8,128)(2,1)} %get-tuple-element.19), calls=%async_computation.2 | async-start | bytes 524288 | tf_op jit(solution)/shard_map/all_to_all | solution.py:154
  85.2 3.2 %collective-permute-start.5 = (bf16[32,2176]{1,0:T(8,128)(2,1)S(1)}, bf16[32,2176]{1,0:T(8,128)(2,1)S(1)}, u32[]{:S(2)}, u32[]{:S(2)}) collective-permute-start(bf16[32,2176]{1,0:T(8,128)(2,1)S(1)} %pad_maximum_fusion.1), channel_id=1, source_target_pairs={{0,24},{8,0},{16,8},{24,16},{1,25},{9,1},{17,9},{25,17},{2,26},{10... | collective-permute-start | bytes 417800 | tf_op jit(solution)/shard_map/ppermute | solution.py:35
  88.4 3.4 %collective-permute-start.4 = (bf16[32,2176]{1,0:T(8,128)(2,1)S(1)}, bf16[32,2176]{1,0:T(8,128)(2,1)S(1)}, u32[]{:S(2)}, u32[]{:S(2)}) collective-permute-start(bf16[32,2176]{1,0:T(8,128)(2,1)S(1)} %pad_maximum_fusion.1), channel_id=1, source_target_pairs={{0,16},{8,24},{16,0},{24,8},{1,17},{9,25},{17,1},{25,9},{2,18},{10... | collective-permute-start | bytes 417800 | tf_op jit(solution)/shard_map/ppermute | solution.py:35
  91.8 1.9 %collective-permute-start.3 = (bf16[32,2176]{1,0:T(8,128)(2,1)S(1)}, bf16[32,2176]{1,0:T(8,128)(2,1)S(1)}, u32[]{:S(2)}, u32[]{:S(2)}) collective-permute-start(bf16[32,2176]{1,0:T(8,128)(2,1)S(1)} %pad_maximum_fusion.1), channel_id=1, source_target_pairs={{0,8},{8,16},{16,24},{24,0},{1,9},{9,17},{17,25},{25,1},{2,10},{10... | collective-permute-start | bytes 417800 | tf_op jit(solution)/shard_map/ppermute | solution.py:35
  93.8 0.0 copy-start.2
  93.8 4.3 %collective-permute-start = (bf16[16,64,256]{2,1,0:T(8,128)(2,1)S(1)}, bf16[16,64,256]{2,1,0:T(8,128)(2,1)S(1)}, u32[]{:S(2)}, u32[]{:S(2)}) collective-permute-start(bf16[16,64,256]{2,1,0:T(8,128)(2,1)S(1)} %slice.27.refs_0_), channel_id=1, source_target_pairs={{0,1},{1,2},{2,3},{3,0},{4,5},{5,6},{6,7},{7,4},{8,9},{9,10},{10,1... | collective-permute-start | bytes 1572872 | tf_op jit(solution)/shard_map/ppermute | solution.py:35
  98.1 2.0 %collective-permute-start.1 = (bf16[16,64,256]{2,1,0:T(8,128)(2,1)S(1)}, bf16[16,64,256]{2,1,0:T(8,128)(2,1)S(1)}, u32[]{:S(2)}, u32[]{:S(2)}) collective-permute-start(bf16[16,64,256]{2,1,0:T(8,128)(2,1)S(1)} %slice.27.refs_0_), channel_id=1, source_target_pairs={{0,2},{1,3},{2,0},{3,1},{4,6},{5,7},{6,4},{7,5},{8,10},{9,11},{10,... | collective-permute-start | bytes 1572872 | tf_op jit(solution)/shard_map/ppermute | solution.py:35
  100.1 0.0 collective-permute-done.5
  100.1 0.0 collective-permute-done.4
  100.1 0.0 collective-permute-done.3
  100.2 0.0 copy-start.1
  100.2 1.9 %collective-permute-start.6 = (bf16[128,2176]{1,0:T(8,128)(2,1)S(1)}, bf16[128,2176]{1,0:T(8,128)(2,1)S(1)}, u32[]{:S(2)}, u32[]{:S(2)}) collective-permute-start(bf16[128,2176]{1,0:T(8,128)(2,1)S(1)} %pad_maximum_fusion.refs_4_), channel_id=1, source_target_pairs={{0,4},{4,0},{1,5},{5,1},{2,6},{6,2},{3,7},{7,3},{8,12},{12,8},{9,1... | collective-permute-start | bytes 1671176 | tf_op jit(solution)/shard_map/ppermute | solution.py:39
  102.1 3.1 %collective-permute-start.2 = (bf16[16,64,256]{2,1,0:T(8,128)(2,1)S(1)}, bf16[16,64,256]{2,1,0:T(8,128)(2,1)}, u32[]{:S(2)}, u32[]{:S(2)}) collective-permute-start(bf16[16,64,256]{2,1,0:T(8,128)(2,1)S(1)} %slice.27.refs_0_), channel_id=1, source_target_pairs={{0,3},{1,0},{2,1},{3,2},{4,7},{5,4},{6,5},{7,6},{8,11},{9,8},{10,9... | collective-permute-start | bytes 1572872 | tf_op jit(solution)/shard_map/ppermute | solution.py:35
  105.3 0.0 all-to-all-done.2.refs_0_
  105.3 0.0 copy-start.3
  105.3 3.9 %collective-permute-start.7 = (bf16[16,32,256]{2,1,0:T(8,128)(2,1)S(1)}, bf16[16,32,256]{2,1,0:T(8,128)(2,1)S(1)}, u32[]{:S(2)}, u32[]{:S(2)}) collective-permute-start(bf16[16,32,256]{2,1,0:T(8,128)(2,1)S(1)} %all-to-all-done.2.refs_0_), channel_id=1, source_target_pairs={{0,1},{1,2},{2,3},{3,0},{4,5},{5,6},{6,7},{7,4},{8,9},{9,10},{10,1... | collective-permute-start | bytes 786440 | tf_op jit(solution)/shard_map/ppermute | solution.py:35
  109.2 9.7 %collective-permute-done.refs_1_ = bf16[16,64,256]{2,1,0:T(8,128)(2,1)S(1)} collective-permute-done((bf16[16,64,256]{2,1,0:T(8,128)(2,1)S(1)}, bf16[16,64,256]{2,1,0:T(8,128)(2,1)S(1)}, u32[]{:S(2)}, u32[]{:S(2)}) %collective-permute-start) | collective-permute-done | bytes 524320 | tf_op jit(solution)/shard_map/ppermute | solution.py:35
  119.0 1.9 %collective-permute-start.8 = (bf16[16,32,256]{2,1,0:T(8,128)(2,1)S(1)}, bf16[16,32,256]{2,1,0:T(8,128)(2,1)}, u32[]{:S(2)}, u32[]{:S(2)}) collective-permute-start(bf16[16,32,256]{2,1,0:T(8,128)(2,1)S(1)} %all-to-all-done.2.refs_0_), channel_id=1, source_target_pairs={{0,2},{1,3},{2,0},{3,1},{4,6},{5,7},{6,4},{7,5},{8,10},{9,11},{10,... | collective-permute-start | bytes 786440 | tf_op jit(solution)/shard_map/ppermute | solution.py:35
  120.9 0.0 collective-permute-done.1.refs_2_
  120.9 0.0 copy-start.6
  120.9 6.9 %collective-permute-start.9 = (bf16[16,32,256]{2,1,0:T(8,128)(2,1)S(1)}, bf16[16,32,256]{2,1,0:T(8,128)(2,1)}, u32[]{:S(2)}, u32[]{:S(2)}) collective-permute-start(bf16[16,32,256]{2,1,0:T(8,128)(2,1)S(1)} %all-to-all-done.2.refs_0_), channel_id=1, source_target_pairs={{0,3},{1,0},{2,1},{3,2},{4,7},{5,4},{6,5},{7,6},{8,11},{9,8},{10,9... | collective-permute-start | bytes 786440 | tf_op jit(solution)/shard_map/ppermute | solution.py:35
  127.9 0.0 collective-permute-done.2.refs_3_
  127.9 0.0 collective-permute-done.6.refs_5_
  127.9 0.0 copy-start.4
  127.9 0.0 copy-done.2
  127.9 0.0 copy-done.1
  127.9 0.0 copy-done.5
  127.9 0.0 copy-done.6
  127.9 0.8 copy-done.4
  128.7 3.6 %shard_map.104 = (bf16[16,4,32,256]{3,2,1,0:T(8,128)(2,1)}, bf16[16,4,32,256]{3,2,1,0:T(8,128)(2,1)}, bf16[256,256]{1,0:T(8,128)(2,1)}) custom-call(s32[1]{0:T(128)} %bitcast.first_ref, s32[1]{0:T(128)} %bitcast.1.expert_ref, bf16[16,64,256]{2,1,0:T(8,128)(2,1)} %copy-done.2, bf16[16,64,256]{2,1,0:T(8,128)(2,1)} %copy-done.5, ...), custom_call_target="tpu_custom_call" | custom-call | tf_op jit(solution)/shard_map/pallas_call | solution.py:165
  132.3 0.0 copy-done.3
  132.3 0.0 collective-permute-done.7.refs_1_
  132.3 0.0 copy-start.7
  132.3 0.9 collective-permute-done.8.refs_2_
  133.3 3.2 %collective-permute-done.9.refs_3_ = bf16[16,32,256]{2,1,0:T(8,128)(2,1)} collective-permute-done((bf16[16,32,256]{2,1,0:T(8,128)(2,1)S(1)}, bf16[16,32,256]{2,1,0:T(8,128)(2,1)}, u32[]{:S(2)}, u32[]{:S(2)}) %collective-permute-start.9) | collective-permute-done | bytes 262176 | tf_op jit(solution)/shard_map/ppermute | solution.py:35
  136.5 0.0 copy-done.7
  136.5 2.9 %shard_map.105 = (bf16[16,4,32,256]{3,2,1,0:T(8,128)(2,1)}, bf16[4,32,2048]{2,1,0:T(8,128)(2,1)}, f32[4,32,2048]{2,1,0:T(8,128)}) custom-call(s32[1]{0:T(128)} %bitcast.first_ref, s32[1]{0:T(128)} %bitcast.3.x_ref, bf16[16,32,256]{2,1,0:T(8,128)(2,1)} %copy-done.3, bf16[16,32,256]{2,1,0:T(8,128)(2,1)} %copy-done.7, ...), custom_call_target="tpu_custom_call" | custom-call | tf_op jit(solution)/shard_map/pallas_call | solution.py:179
  139.4 1.9 %collective-permute-start.10 = (bf16[4,32,2048]{2,1,0:T(8,128)(2,1)}, bf16[4,32,2048]{2,1,0:T(8,128)(2,1)S(1)}, u32[]{:S(2)}, u32[]{:S(2)}) collective-permute-start(bf16[4,32,2048]{2,1,0:T(8,128)(2,1)} %get-tuple-element.23), channel_id=1, source_target_pairs={{0,4},{4,0},{1,5},{5,1},{2,6},{6,2},{3,7},{7,3},{8,12},{12,8},{9,1... | collective-permute-start | bytes 1572872 | tf_op jit(solution)/shard_map/ppermute | solution.py:39
  141.4 2.1 %collective-permute-done.10 = bf16[4,32,2048]{2,1,0:T(8,128)(2,1)S(1)} collective-permute-done((bf16[4,32,2048]{2,1,0:T(8,128)(2,1)}, bf16[4,32,2048]{2,1,0:T(8,128)(2,1)S(1)}, u32[]{:S(2)}, u32[]{:S(2)}) %collective-permute-start.10) | collective-permute-done | bytes 524320 | tf_op jit(solution)/shard_map/ppermute | solution.py:39
  143.4 1.3 add_convert_fusion
  144.8 13.5 %all_to_all.26 = bf16[4,32,2048]{2,1,0:T(8,128)(2,1)S(1)} all-to-all(bf16[4,32,2048]{2,1,0:T(8,128)(2,1)S(1)} %add_convert_fusion), channel_id=1, replica_groups=mesh['z'=16,'x'=4,'c'=2,'y'=4] {'x'}, dimensions={0} | all-to-all | bytes 1048576 | tf_op jit(solution)/shard_map/all_to_all | solution.py:194
  158.3 0.1 reduce_sum.44
  158.3 0.1 reshape.71
  158.4 25.5 %all_to_all.27 = bf16[16,2,2048]{2,1,0:T(2,128)(2,1)S(1)} all-to-all(bf16[16,2,2048]{2,1,0:T(2,128)(2,1)S(1)} %reshape.71), channel_id=1, replica_groups=mesh['z'=16,'x'=4,'c'=2,'y'=4] {'z'}, dimensions={0} | all-to-all | bytes 262144 | tf_op jit(solution)/shard_map/all_to_all | solution.py:196
  183.9 0.7 reduce_sum.45
  (11 shorter events, 0.2 us)
Async XLA Ops:
  3.0 9.3 %copy-start.8 = (bf16[2,2048]{1,0:T(2,128)(2,1)S(1)}, bf16[2,2048]{1,0:T(2,128)(2,1)}, u32[]{:S(2)}) copy-start(bf16[2,2048]{1,0:T(2,128)(2,1)} %param.7) | copy-start | bytes 24580
  3.0 9.8 %copy-start.9 = (s32[2,2]{1,0:T(2,128)S(1)}, s32[2,2]{1,0:T(2,128)}, u32[]{:S(2)}) copy-start(s32[2,2]{1,0:T(2,128)} %param.8) | copy-start | bytes 52
  3.0 9.9 %copy-start.10 = (f32[2,2]{1,0:T(2,128)S(1)}, f32[2,2]{1,0:T(2,128)}, u32[]{:S(2)}) copy-start(f32[2,2]{1,0:T(2,128)} %param.9) | copy-start | bytes 52
  3.0 21.9 %all-to-all-start = ((bf16[32,3,16,256]{3,2,1,0:T(8,128)(2,1)}), bf16[32,3,16,256]{3,2,1,0:T(8,128)(2,1)S(1)}, u32[]{:S(2)}, u32[]{:S(2)}) async-start(bf16[32,3,16,256]{3,2,1,0:T(8,128)(2,1)} %bitcast.12), calls=%async_computation | async-start | bytes 1572864 | tf_op jit(solution)/shard_map/all_to_all | solution.py:129
  24.9 0.9 copy-start
  80.0 25.3 %all-to-all-start.2 = ((bf16[16,32,256]{2,1,0:T(8,128)(2,1)}), bf16[16,32,256]{2,1,0:T(8,128)(2,1)S(1)}, u32[]{:S(2)}, u32[]{:S(2)}) async-start(bf16[16,32,256]{2,1,0:T(8,128)(2,1)} %get-tuple-element.19), calls=%async_computation.2 | async-start | bytes 524288 | tf_op jit(solution)/shard_map/all_to_all | solution.py:154
  85.2 15.0 %collective-permute-start.5 = (bf16[32,2176]{1,0:T(8,128)(2,1)S(1)}, bf16[32,2176]{1,0:T(8,128)(2,1)S(1)}, u32[]{:S(2)}, u32[]{:S(2)}) collective-permute-start(bf16[32,2176]{1,0:T(8,128)(2,1)S(1)} %pad_maximum_fusion.1), channel_id=1, source_target_pairs={{0,24},{8,0},{16,8},{24,16},{1,25},{9,1},{17,9},{25,17},{2,26},{10... | collective-permute-start | bytes 417800 | tf_op jit(solution)/shard_map/ppermute | solution.py:35
  88.4 11.8 %collective-permute-start.4 = (bf16[32,2176]{1,0:T(8,128)(2,1)S(1)}, bf16[32,2176]{1,0:T(8,128)(2,1)S(1)}, u32[]{:S(2)}, u32[]{:S(2)}) collective-permute-start(bf16[32,2176]{1,0:T(8,128)(2,1)S(1)} %pad_maximum_fusion.1), channel_id=1, source_target_pairs={{0,16},{8,24},{16,0},{24,8},{1,17},{9,25},{17,1},{25,9},{2,18},{10... | collective-permute-start | bytes 417800 | tf_op jit(solution)/shard_map/ppermute | solution.py:35
  91.8 8.4 %collective-permute-start.3 = (bf16[32,2176]{1,0:T(8,128)(2,1)S(1)}, bf16[32,2176]{1,0:T(8,128)(2,1)S(1)}, u32[]{:S(2)}, u32[]{:S(2)}) collective-permute-start(bf16[32,2176]{1,0:T(8,128)(2,1)S(1)} %pad_maximum_fusion.1), channel_id=1, source_target_pairs={{0,8},{8,16},{16,24},{24,0},{1,9},{9,17},{17,25},{25,1},{2,10},{10... | collective-permute-start | bytes 417800 | tf_op jit(solution)/shard_map/ppermute | solution.py:35
  93.8 34.1 %copy-start.2 = (bf16[16,64,256]{2,1,0:T(8,128)(2,1)}, bf16[16,64,256]{2,1,0:T(8,128)(2,1)S(1)}, u32[]{:S(2)}) copy-start(bf16[16,64,256]{2,1,0:T(8,128)(2,1)S(1)} %slice.27.refs_0_) | copy-start | bytes 1572868
  93.8 25.2 %collective-permute-start = (bf16[16,64,256]{2,1,0:T(8,128)(2,1)S(1)}, bf16[16,64,256]{2,1,0:T(8,128)(2,1)S(1)}, u32[]{:S(2)}, u32[]{:S(2)}) collective-permute-start(bf16[16,64,256]{2,1,0:T(8,128)(2,1)S(1)} %slice.27.refs_0_), channel_id=1, source_target_pairs={{0,1},{1,2},{2,3},{3,0},{4,5},{5,6},{6,7},{7,4},{8,9},{9,10},{10,1... | collective-permute-start | bytes 1572872 | tf_op jit(solution)/shard_map/ppermute | solution.py:35
  98.1 22.8 %collective-permute-start.1 = (bf16[16,64,256]{2,1,0:T(8,128)(2,1)S(1)}, bf16[16,64,256]{2,1,0:T(8,128)(2,1)S(1)}, u32[]{:S(2)}, u32[]{:S(2)}) collective-permute-start(bf16[16,64,256]{2,1,0:T(8,128)(2,1)S(1)} %slice.27.refs_0_), channel_id=1, source_target_pairs={{0,2},{1,3},{2,0},{3,1},{4,6},{5,7},{6,4},{7,5},{8,10},{9,11},{10,... | collective-permute-start | bytes 1572872 | tf_op jit(solution)/shard_map/ppermute | solution.py:35
  100.2 27.7 %copy-start.1 = (bf16[128,2176]{1,0:T(8,128)(2,1)}, bf16[128,2176]{1,0:T(8,128)(2,1)S(1)}, u32[]{:S(2)}) copy-start(bf16[128,2176]{1,0:T(8,128)(2,1)S(1)} %pad_maximum_fusion.refs_4_) | copy-start | bytes 1671172
  100.2 27.7 %collective-permute-start.6 = (bf16[128,2176]{1,0:T(8,128)(2,1)S(1)}, bf16[128,2176]{1,0:T(8,128)(2,1)S(1)}, u32[]{:S(2)}, u32[]{:S(2)}) collective-permute-start(bf16[128,2176]{1,0:T(8,128)(2,1)S(1)} %pad_maximum_fusion.refs_4_), channel_id=1, source_target_pairs={{0,4},{4,0},{1,5},{5,1},{2,6},{6,2},{3,7},{7,3},{8,12},{12,8},{9,1... | collective-permute-start | bytes 1671176 | tf_op jit(solution)/shard_map/ppermute | solution.py:39
  102.1 25.7 %collective-permute-start.2 = (bf16[16,64,256]{2,1,0:T(8,128)(2,1)S(1)}, bf16[16,64,256]{2,1,0:T(8,128)(2,1)}, u32[]{:S(2)}, u32[]{:S(2)}) collective-permute-start(bf16[16,64,256]{2,1,0:T(8,128)(2,1)S(1)} %slice.27.refs_0_), channel_id=1, source_target_pairs={{0,3},{1,0},{2,1},{3,2},{4,7},{5,4},{6,5},{7,6},{8,11},{9,8},{10,9... | collective-permute-start | bytes 1572872 | tf_op jit(solution)/shard_map/ppermute | solution.py:35
  105.3 27.0 %copy-start.3 = (bf16[16,32,256]{2,1,0:T(8,128)(2,1)}, bf16[16,32,256]{2,1,0:T(8,128)(2,1)S(1)}, u32[]{:S(2)}) copy-start(bf16[16,32,256]{2,1,0:T(8,128)(2,1)S(1)} %all-to-all-done.2.refs_0_) | copy-start | bytes 786436
  105.3 27.0 %collective-permute-start.7 = (bf16[16,32,256]{2,1,0:T(8,128)(2,1)S(1)}, bf16[16,32,256]{2,1,0:T(8,128)(2,1)S(1)}, u32[]{:S(2)}, u32[]{:S(2)}) collective-permute-start(bf16[16,32,256]{2,1,0:T(8,128)(2,1)S(1)} %all-to-all-done.2.refs_0_), channel_id=1, source_target_pairs={{0,1},{1,2},{2,3},{3,0},{4,5},{5,6},{6,7},{7,4},{8,9},{9,10},{10,1... | collective-permute-start | bytes 786440 | tf_op jit(solution)/shard_map/ppermute | solution.py:35
  119.0 9.0 %copy-start.5 = (bf16[16,64,256]{2,1,0:T(8,128)(2,1)}, bf16[16,64,256]{2,1,0:T(8,128)(2,1)S(1)}, u32[]{:S(2)}) copy-start(bf16[16,64,256]{2,1,0:T(8,128)(2,1)S(1)} %collective-permute-done.refs_1_) | copy-start | bytes 1572868
  119.0 14.3 %collective-permute-start.8 = (bf16[16,32,256]{2,1,0:T(8,128)(2,1)S(1)}, bf16[16,32,256]{2,1,0:T(8,128)(2,1)}, u32[]{:S(2)}, u32[]{:S(2)}) collective-permute-start(bf16[16,32,256]{2,1,0:T(8,128)(2,1)S(1)} %all-to-all-done.2.refs_0_), channel_id=1, source_target_pairs={{0,2},{1,3},{2,0},{3,1},{4,6},{5,7},{6,4},{7,5},{8,10},{9,11},{10,... | collective-permute-start | bytes 786440 | tf_op jit(solution)/shard_map/ppermute | solution.py:35
  120.9 7.0 %copy-start.6 = (bf16[16,64,256]{2,1,0:T(8,128)(2,1)}, bf16[16,64,256]{2,1,0:T(8,128)(2,1)S(1)}, u32[]{:S(2)}) copy-start(bf16[16,64,256]{2,1,0:T(8,128)(2,1)S(1)} %collective-permute-done.1.refs_2_) | copy-start | bytes 1572868
  120.9 15.6 %collective-permute-start.9 = (bf16[16,32,256]{2,1,0:T(8,128)(2,1)S(1)}, bf16[16,32,256]{2,1,0:T(8,128)(2,1)}, u32[]{:S(2)}, u32[]{:S(2)}) collective-permute-start(bf16[16,32,256]{2,1,0:T(8,128)(2,1)S(1)} %all-to-all-done.2.refs_0_), channel_id=1, source_target_pairs={{0,3},{1,0},{2,1},{3,2},{4,7},{5,4},{6,5},{7,6},{8,11},{9,8},{10,9... | collective-permute-start | bytes 786440 | tf_op jit(solution)/shard_map/ppermute | solution.py:35
  127.9 0.8 copy-start.4
  132.3 4.2 %copy-start.7 = (bf16[16,32,256]{2,1,0:T(8,128)(2,1)}, bf16[16,32,256]{2,1,0:T(8,128)(2,1)S(1)}, u32[]{:S(2)}) copy-start(bf16[16,32,256]{2,1,0:T(8,128)(2,1)S(1)} %collective-permute-done.7.refs_1_) | copy-start | bytes 786436
  139.4 4.0 %collective-permute-start.10 = (bf16[4,32,2048]{2,1,0:T(8,128)(2,1)}, bf16[4,32,2048]{2,1,0:T(8,128)(2,1)S(1)}, u32[]{:S(2)}, u32[]{:S(2)}) collective-permute-start(bf16[4,32,2048]{2,1,0:T(8,128)(2,1)} %get-tuple-element.23), channel_id=1, source_target_pairs={{0,4},{4,0},{1,5},{5,1},{2,6},{6,2},{3,7},{7,3},{8,12},{12,8},{9,1... | collective-permute-start | bytes 1572872 | tf_op jit(solution)/shard_map/ppermute | solution.py:39
where the time goes:
time: 186 us; the launch traced here: 185 us
  blocking collectives  90.9 us (49%)
  starting transfers between devices  49 us (26%)
  waiting for transfers between devices  27 us (15%)
  Pallas kernels  11.1 us (6%)
  other arithmetic  3.49 us (2%)
  local copies, waits for them, and re-layouts  2.1 us (1%)
    all_to_all x1, blocking collectives, per_device(): first = lax.all_to_all(early, 'z', 0, 0, tiled=True)  51.9 us
    ppermute x9, starting transfers between devices, shift(): lax.ppermute(array, axis, [(i, (i + by) % size) for i in range(size)])  30.8 us
    all_to_all x1, blocking collectives, per_device(): lax.all_to_all(by_x, 'z', 0, 0, tiled=True).astype(jnp.float32).sum(axis=0)  25.5 us
    ppermute x9, waiting for transfers between devices, shift(): lax.ppermute(array, axis, [(i, (i + by) % size) for i in range(size)])  13.9 us
    all_to_all x1, blocking collectives, per_device(): lax.all_to_all(chip, 'x', 0, 0, tiled=True).astype(jnp.float32).sum(axis=0)  13.5 us
    all_to_all x1, waiting for transfers between devices, per_device(): lax.all_to_all(local.reshape(XC * NY, 3, depth, block), ('x', 'c', 'y'),...  11 us
    all_to_all x1, starting transfers between devices, per_device(): lax.all_to_all(local.reshape(XC * NY, 3, depth, block), ('x', 'c', 'y'),...  9.28 us
    all_to_all x1, starting transfers between devices, per_device(): second = lax.all_to_all(late, 'z', 0, 0, tiled=True)  5.17 us
  transfers between devices with their start and end apart: 13, of which 5 were waited for; matrix products, arithmetic and copies ran while one was open for 1% of the time, Pallas kernels for 2%

commit v1 on v0

--- a/solution.py
+++ b/solution.py
@@ -55,17 +55,17 @@
             out[s, y, 2] = down[e, :, cut].astype(jnp.bfloat16)
 
 
-def sort_kernel(y_ref, swapped, riders, early, late):
-    depth = swapped.shape[3]
+def sort_kernel(y_ref, swapped, riders, out):
+    kinds, depth = swapped.shape[2:4]
     for e in range(NZ // NY):
         x = lax.rem(NX + e - y_ref[0], NX)
         for y in range(NY):
-            for c in range(NC):
-                part = swapped[NC * x + c, y]
-                early[NY * e + y, depth * c : depth * (c + 1)] = part[0]
-                early[NY * e + y, depth * (NC + c) : depth * (NC + c + 1)] = part[1]
-                late[NY * e + y, depth * c : depth * (c + 1)] = part[2]
-            early[NY * e + y, 2 * NC * depth :] = riders[...]
+            at = 0
+            for m in range(kinds):
+                for c in range(NC):
+                    out[NY * e + y, at : at + depth] = swapped[NC * x + c, y, m]
+                    at += depth
+            out[NY * e + y, at:] = riders[...]
 
 
 def put(first_ref, ins, outs):
@@ -76,8 +76,11 @@
             out[:, at] = part[:, m * span : (m + 1) * span]
 
 
-def all_y(own):
-    return [own] + [shift(own, "y", k, NY) for k in range(1, NY)]
+def all_from(own, axis, size):
+    got = [own]
+    for k in range(1, size):
+        got.append(shift(own, axis, k, size))
+    return got
 
 
 def hidden_kernel(first_ref, expert_ref, *refs):
@@ -110,22 +113,38 @@
         theirs[to] = both[1, k].astype(jnp.bfloat16)
 
 
+def on_core(kernel, scalars, arrays, outs, scratch=(), limit=None):
+    smem, vmem = pl.BlockSpec(memory_space=pltpu.SMEM), pl.BlockSpec(memory_space=pltpu.VMEM)
+    return pl.pallas_call(
+        kernel,
+        out_shape=outs,
+        in_specs=[smem] * len(scalars) + [vmem] * len(arrays),
+        out_specs=[vmem] * len(outs),
+        scratch_shapes=scratch,
+        compiler_params=pltpu.CompilerParams(vmem_limit_bytes=limit),
+    )(*scalars, *arrays)
+
+
+def held(array):
+    return pltpu.with_memory_space_constraint(array, pltpu.VMEM)
+
+
 def per_device(tokens, route_experts, route_logits, norm_gain, gate_train, up_train, down_train):
     experts, depth, wide = gate_train.shape
     own_rows, width = tokens.shape
     block = wide // XC
-    smem, vmem = pl.BlockSpec(memory_space=pltpu.SMEM), pl.BlockSpec(memory_space=pltpu.VMEM)
     y, x = lax.axis_index("y"), lax.axis_index("x")
     expert = lax.axis_index("z") // (NZ // experts)
     first_block = lax.rem(NX + expert - y, NX).reshape(1).astype(jnp.int32)
     expert, y, x = (i.reshape(1).astype(jnp.int32) for i in (expert, y, x))
 
-    local = pl.pallas_call(
+    bf16, f32 = jnp.bfloat16, jnp.float32
+    (local,) = on_core(
         pack_kernel,
-        out_shape=jax.ShapeDtypeStruct((XC, NY, 3, depth, block), jnp.bfloat16),
-        in_specs=[smem] + [vmem] * 4,
-        out_specs=vmem,
-    )(x, norm_gain[None, :], gate_train, up_train, down_train)
+        (x,),
+        (norm_gain[None, :], gate_train, up_train, down_train),
+        [pltpu.VMEM((XC, NY, 3, depth, block), bf16)],
+    )
     swapped = lax.all_to_all(
         local.reshape(XC * NY, 3, depth, block), ("x", "c", "y"), 0, 0, tiled=True
     )
@@ -140,52 +159,45 @@
         ]
     )
     span = NC * depth
-    early, late = pl.pallas_call(
+    cut = 3 * span
+    (sorted_by_z,) = on_core(
         sort_kernel,
-        out_shape=[
-            jax.ShapeDtypeStruct((NZ, 2 * span + spread + 8, block), jnp.bfloat16),
-            jax.ShapeDtypeStruct((NZ, span, block), jnp.bfloat16),
-        ],
-        in_specs=[smem, vmem, vmem],
-        out_specs=[vmem, vmem],
-    )(y, swapped.reshape(XC, NY, 3, depth, block), riders)
-    first = lax.all_to_all(early, "z", 0, 0, tiled=True)
-    first, late = lax.optimization_barrier((first, late))
-    second = lax.all_to_all(late, "z", 0, 0, tiled=True)
-
-    cut = 2 * span
-    parts = all_y(first[:, :cut])
+        (y,),
+        (held(swapped.reshape(XC, NY, 3, depth, block)), held(riders)),
+        [pltpu.VMEM((NZ, cut + spread + 8, block), bf16)],
+        limit=8 << 20,
+    )
+    first = lax.all_to_all(sorted_by_z, "z", 0, 0, tiled=True)
+
+    parts = all_from(first[:, : 2 * span], "y", NY)
     rows_z = first[:, cut : cut + spread].reshape(NZ * own_rows, width)
     table_z = first[:, cut + spread : cut + spread + own_rows, :PAD]
     rows_z = jnp.concatenate([rows_z, table_z.reshape(NZ * own_rows, PAD)], axis=1)
-    rows_x = [rows_z] + [shift(rows_z, "x", k, NX) for k in range(1, NX)]
+    rows_x = all_from(rows_z, "x", NX)
     rows_x = jnp.concatenate(rows_x)
     rows_c = swap_core(rows_x)
-    placed = jax.ShapeDtypeStruct((NZ, NX, span, block), jnp.bfloat16)
-    gate_serve, up_serve, hidden = pl.pallas_call(
+    placed = jax.ShapeDtypeStruct((NZ, NX, span, block), bf16)
+    half = rows_x.shape[0]
+    gate_serve, up_serve, hidden = on_core(
         hidden_kernel,
-        out_shape=[
+        (first_block, expert),
+        (*parts, rows_x, rows_c),
+        [placed, placed, pltpu.VMEM((2 * half, block), bf16)],
+        [pltpu.VMEM((2 * half, width + PAD), bf16)],
+    )
+
+    parts = all_from(first[:, 2 * span : cut], "y", NY)
+    down_serve, theirs, mine = on_core(
+        down_kernel,
+        (first_block, x),
+        [held(a) for a in (*parts, hidden)],
+        [
             placed,
-            placed,
-            jax.ShapeDtypeStruct((2 * rows_x.shape[0], block), jnp.bfloat16),
+            pltpu.VMEM((NX, half // NX, width), bf16),
+            pltpu.VMEM((NX, half // NX, width), f32),
         ],
-        in_specs=[smem, smem] + [vmem] * (len(parts) + 2),
-        out_specs=[vmem] * 3,
-        scratch_shapes=[pltpu.VMEM((2 * rows_x.shape[0], width + PAD), jnp.bfloat16)],
-    )(first_block, expert, *parts, rows_x, rows_c)
-
-    parts = all_y(second)
-    half = rows_x.shape[0]
-    down_serve, theirs, mine = pl.pallas_call(
-        down_kernel,
-        out_shape=[
-            placed,
-            jax.ShapeDtypeStruct((NX, half // NX, width), jnp.bfloat16),
-            jax.ShapeDtypeStruct((NX, half // NX, width), jnp.float32),
-        ],
-        in_specs=[smem, smem] + [vmem] * (len(parts) + 1),
-        out_specs=[vmem] * 3,
-    )(first_block, x, *parts, hidden)
+        limit=16 << 20,
+    )
     gate_serve, up_serve, down_serve = (
         matrix.reshape(1, width, block) for matrix in (gate_serve, up_serve, down_serve)
     )

time: 186 us -> 179 us (0.962)
  blocking collectives: 90.9 us -> 97.9 us
  starting transfers between devices: 49 us -> 45.1 us
  Pallas kernels: 11.1 us -> 7.39 us
  waiting for transfers between devices: 27 us -> 23.4 us
    all_to_all x1, blocking collectives: 51.9 us -> 62.5 us  [per_device(): first = lax.all_to_all(sorted_by_z, 'z', 0, 0, tiled=True)]
    all_to_all x1 -> x0, starting transfers between devices: 5.17 us -> none  [per_device(): second = lax.all_to_all(late, 'z', 0, 0, tiled=True)]
    ppermute x9, waiting for transfers between devices: 13.9 us -> 9.92 us  [shift(): lax.ppermute(array, axis, [(i, (i + by) % size) for i in range(size)])]
    pallas_call x4, Pallas kernels: 11.1 us -> 7.39 us  [on_core(): pl.pallas_call(kernel, out_shape=outs, in_specs=[smem] * len(scalars) + [...]
    all_to_all x1, blocking collectives: 25.5 us -> 23 us  [per_device(): lax.all_to_all(by_x, 'z', 0, 0, tiled=True).astype(jnp.float32).sum(axis=0)]
  transfers between devices with their start and end apart: 13 -> 12, of which waited for: 5 -> 6; matrix products, arithmetic and copies ran while one was open for 1% -> 1% of each run, Pallas kernels for 2% -> 2%
where the time goes in v1:
time: 179 us; the launch traced here: 178 us
  blocking collectives  97.9 us (55%)
  starting transfers between devices  45.1 us (25%)
  waiting for transfers between devices  23.4 us (13%)
  Pallas kernels  7.39 us (4%)
  local copies, waits for them, and re-layouts  2.02 us (1%)
    all_to_all x1, blocking collectives, per_device(): first = lax.all_to_all(sorted_by_z, 'z', 0, 0, tiled=True)  62.5 us
    ppermute x9, starting transfers between devices, shift(): lax.ppermute(array, axis, [(i, (i + by) % size) for i in range(size)])  31.9 us
    all_to_all x1, blocking collectives, per_device(): lax.all_to_all(by_x, 'z', 0, 0, tiled=True).astype(jnp.float32).sum(axis=0)  23 us
    all_to_all x1, blocking collectives, per_device(): lax.all_to_all(chip, 'x', 0, 0, tiled=True).astype(jnp.float32).sum(axis=0)  12.5 us
    all_to_all x1, waiting for transfers between devices, per_device(): lax.all_to_all(local.reshape(XC * NY, 3, depth, block), ('x', 'c', 'y'),...  11.6 us
    ppermute x9, waiting for transfers between devices, shift(): lax.ppermute(array, axis, [(i, (i + by) % size) for i in range(size)])  9.92 us
    all_to_all x1, starting transfers between devices, per_device(): lax.all_to_all(local.reshape(XC * NY, 3, depth, block), ('x', 'c', 'y'),...  9.28 us
    pallas_call x4, Pallas kernels, on_core(): pl.pallas_call(kernel, out_shape=outs, in_specs=[smem] * len(scalars) + [...  7.39 us
  transfers between devices with their start and end apart: 12, of which 6 were waited for; matrix products, arithmetic and copies ran while one was open for 1% of the time, Pallas kernels for 2%

profile of v1, /device:TPU:24, one launch (start us, length us, event | category | flops | bytes accessed | tf_op | source)
XLA Modules:
  0.0 178.4 jit_solution(5576075679315886038)
XLA Ops:
  0.6 2.4 %shard_map.102 = bf16[8,4,3,16,256]{4,3,2,1,0:T(8,128)(2,1)} custom-call(s32[1]{0:T(128)} %bitcast.3.x_ref, f32[1,16]{1,0:T(1,128)} %bitcast.14, f32[4,16,2048]{2,1,0:T(8,128)} %gate.1, f32[4,16,2048]{2,1,0:T(8,128)} %up.1, f32[4,16,2048]{2,1,0:T(8,128)} %down.1), custom_call_target="tpu_custom_call" | custom-call | tf_op jit(solution)/shard_map/pallas_call | solution.py:118
  3.0 0.0 copy-start.5
  3.0 0.0 copy-start.6
  3.0 0.0 copy-start.7
  3.0 9.3 %all-to-all-start = ((bf16[32,3,16,256]{3,2,1,0:T(8,128)(2,1)}), bf16[32,3,16,256]{3,2,1,0:T(8,128)(2,1)S(1)}, u32[]{:S(2)}, u32[]{:S(2)}) async-start(bf16[32,3,16,256]{3,2,1,0:T(8,128)(2,1)} %bitcast.5), calls=%async_computation | async-start | bytes 1572864 | tf_op jit(solution)/shard_map/all_to_all | solution.py:148
  12.3 0.0 copy-done.5
  12.3 0.1 convert_reduce_fusion
  12.5 0.2 fusion.3
  12.7 0.1 fusion.4
  12.8 0.0 copy-done.6
  12.8 0.2 slice_reduce_fusion.1
  13.0 0.0 copy-done.7
  13.0 0.2 fusion.8
  13.2 0.1 fusion.7
  13.3 11.6 %all-to-all-done = bf16[32,3,16,256]{3,2,1,0:T(8,128)(2,1)S(1)} async-done(((bf16[32,3,16,256]{3,2,1,0:T(8,128)(2,1)}), bf16[32,3,16,256]{3,2,1,0:T(8,128)(2,1)S(1)}, u32[]{:S(2)}, u32[]{:S(2)}) %all-to-all-start) | async-done | bytes 786464 | tf_op jit(solution)/shard_map/all_to_all | solution.py:148
  24.9 0.1 shard_map.103
  25.0 62.5 %all_to_all.20 = bf16[16,120,256]{2,1,0:T(8,128)(2,1)S(1)} all-to-all(bf16[16,120,256]{2,1,0:T(8,128)(2,1)S(1)} %shard_map.103), channel_id=1, replica_groups=mesh['z'=16,'x'=4,'c'=2,'y'=4] {'z'}, dimensions={0} | all-to-all | bytes 1966080 | tf_op jit(solution)/shard_map/all_to_all | solution.py:170
  87.5 0.1 reshape.66
  87.6 2.6 %collective-permute-start.3 = (bf16[32,2176]{1,0:T(8,128)(2,1)S(1)}, bf16[32,2176]{1,0:T(8,128)(2,1)S(1)}, u32[]{:S(2)}, u32[]{:S(2)}) collective-permute-start(bf16[32,2176]{1,0:T(8,128)(2,1)S(1)} %pad_maximum_fusion.1), channel_id=1, source_target_pairs={{0,8},{8,16},{16,24},{24,0},{1,9},{9,17},{17,25},{25,1},{2,10},{10... | collective-permute-start | bytes 417800 | tf_op jit(solution)/shard_map/ppermute | solution.py:35
  90.2 3.8 %collective-permute-start.4 = (bf16[32,2176]{1,0:T(8,128)(2,1)S(1)}, bf16[32,2176]{1,0:T(8,128)(2,1)S(1)}, u32[]{:S(2)}, u32[]{:S(2)}) collective-permute-start(bf16[32,2176]{1,0:T(8,128)(2,1)S(1)} %pad_maximum_fusion.1), channel_id=1, source_target_pairs={{0,16},{8,24},{16,0},{24,8},{1,17},{9,25},{17,1},{25,9},{2,18},{10... | collective-permute-start | bytes 417800 | tf_op jit(solution)/shard_map/ppermute | solution.py:35
  93.9 2.7 %collective-permute-start.5 = (bf16[32,2176]{1,0:T(8,128)(2,1)S(1)}, bf16[32,2176]{1,0:T(8,128)(2,1)S(1)}, u32[]{:S(2)}, u32[]{:S(2)}) collective-permute-start(bf16[32,2176]{1,0:T(8,128)(2,1)S(1)} %pad_maximum_fusion.1), channel_id=1, source_target_pairs={{0,24},{8,0},{16,8},{24,16},{1,25},{9,1},{17,9},{25,17},{2,26},{10... | collective-permute-start | bytes 417800 | tf_op jit(solution)/shard_map/ppermute | solution.py:35
  96.7 0.0 copy-start.1
  96.8 5.0 %collective-permute-start = (bf16[16,64,256]{2,1,0:T(8,128)(2,1)S(1)}, bf16[16,64,256]{2,1,0:T(8,128)(2,1)S(1)}, u32[]{:S(2)}, u32[]{:S(2)}) collective-permute-start(bf16[16,64,256]{2,1,0:T(8,128)(2,1)S(1)} %slice.34.refs_0_), channel_id=1, source_target_pairs={{0,1},{1,2},{2,3},{3,0},{4,5},{5,6},{6,7},{7,4},{8,9},{9,10},{10,1... | collective-permute-start | bytes 1572872 | tf_op jit(solution)/shard_map/ppermute | solution.py:35
  101.8 1.9 %collective-permute-start.1 = (bf16[16,64,256]{2,1,0:T(8,128)(2,1)S(1)}, bf16[16,64,256]{2,1,0:T(8,128)(2,1)S(1)}, u32[]{:S(2)}, u32[]{:S(2)}) collective-permute-start(bf16[16,64,256]{2,1,0:T(8,128)(2,1)S(1)} %slice.34.refs_0_), channel_id=1, source_target_pairs={{0,2},{1,3},{2,0},{3,1},{4,6},{5,7},{6,4},{7,5},{8,10},{9,11},{10,... | collective-permute-start | bytes 1572872 | tf_op jit(solution)/shard_map/ppermute | solution.py:35
  103.7 0.0 collective-permute-done.3
  103.7 0.0 collective-permute-done.4
  103.7 0.0 collective-permute-done.5
  103.8 0.0 copy-start
  103.8 1.9 %collective-permute-start.6 = (bf16[128,2176]{1,0:T(8,128)(2,1)S(1)}, bf16[128,2176]{1,0:T(8,128)(2,1)S(1)}, u32[]{:S(2)}, u32[]{:S(2)}) collective-permute-start(bf16[128,2176]{1,0:T(8,128)(2,1)S(1)} %pad_maximum_fusion.refs_4_), channel_id=1, source_target_pairs={{0,4},{4,0},{1,5},{5,1},{2,6},{6,2},{3,7},{7,3},{8,12},{12,8},{9,1... | collective-permute-start | bytes 1671176 | tf_op jit(solution)/shard_map/ppermute | solution.py:39
  105.7 3.2 %collective-permute-start.2 = (bf16[16,64,256]{2,1,0:T(8,128)(2,1)S(1)}, bf16[16,64,256]{2,1,0:T(8,128)(2,1)}, u32[]{:S(2)}, u32[]{:S(2)}) collective-permute-start(bf16[16,64,256]{2,1,0:T(8,128)(2,1)S(1)} %slice.34.refs_0_), channel_id=1, source_target_pairs={{0,3},{1,0},{2,1},{3,2},{4,7},{5,4},{6,5},{7,6},{8,11},{9,8},{10,9... | collective-permute-start | bytes 1572872 | tf_op jit(solution)/shard_map/ppermute | solution.py:35
  108.9 3.9 %collective-permute-start.7 = (bf16[16,32,256]{2,1,0:T(8,128)(2,1)S(1)}, bf16[16,32,256]{2,1,0:T(8,128)(2,1)S(1)}, u32[]{:S(2)}, u32[]{:S(2)}) collective-permute-start(bf16[16,32,256]{2,1,0:T(8,128)(2,1)S(1)} %slice.37.refs_0_), channel_id=1, source_target_pairs={{0,1},{1,2},{2,3},{3,0},{4,5},{5,6},{6,7},{7,4},{8,9},{9,10},{10,1... | collective-permute-start | bytes 786440 | tf_op jit(solution)/shard_map/ppermute | solution.py:35
  112.8 4.3 %collective-permute-done.refs_1_ = bf16[16,64,256]{2,1,0:T(8,128)(2,1)S(1)} collective-permute-done((bf16[16,64,256]{2,1,0:T(8,128)(2,1)S(1)}, bf16[16,64,256]{2,1,0:T(8,128)(2,1)S(1)}, u32[]{:S(2)}, u32[]{:S(2)}) %collective-permute-start) | collective-permute-done | bytes 524320 | tf_op jit(solution)/shard_map/ppermute | solution.py:35
  117.2 0.0 copy-start.3
  117.2 1.9 %collective-permute-start.8 = (bf16[16,32,256]{2,1,0:T(8,128)(2,1)S(1)}, bf16[16,32,256]{2,1,0:T(8,128)(2,1)S(1)}, u32[]{:S(2)}, u32[]{:S(2)}) collective-permute-start(bf16[16,32,256]{2,1,0:T(8,128)(2,1)S(1)} %slice.37.refs_0_), channel_id=1, source_target_pairs={{0,2},{1,3},{2,0},{3,1},{4,6},{5,7},{6,4},{7,5},{8,10},{9,11},{10,... | collective-permute-start | bytes 786440 | tf_op jit(solution)/shard_map/ppermute | solution.py:35
  119.1 0.0 collective-permute-done.1.refs_2_
  119.1 0.0 copy-start.4
  119.1 0.8 copy-done.4
  119.9 6.9 %collective-permute-start.9 = (bf16[16,32,256]{2,1,0:T(8,128)(2,1)S(1)}, bf16[16,32,256]{2,1,0:T(8,128)(2,1)S(1)}, u32[]{:S(2)}, u32[]{:S(2)}) collective-permute-start(bf16[16,32,256]{2,1,0:T(8,128)(2,1)S(1)} %slice.37.refs_0_), channel_id=1, source_target_pairs={{0,3},{1,0},{2,1},{3,2},{4,7},{5,4},{6,5},{7,6},{8,11},{9,8},{10,9... | collective-permute-start | bytes 786440 | tf_op jit(solution)/shard_map/ppermute | solution.py:35
  126.8 0.8 collective-permute-done.2.refs_3_
  127.6 0.0 collective-permute-done.6.refs_5_
  127.6 0.0 copy-start.2
  127.6 0.0 copy-done.1
  127.6 0.0 copy-done
  127.6 0.0 copy-done.3
  127.6 0.8 copy-done.2
  128.4 3.6 %shard_map.104 = (bf16[16,4,32,256]{3,2,1,0:T(8,128)(2,1)}, bf16[16,4,32,256]{3,2,1,0:T(8,128)(2,1)}, bf16[256,256]{1,0:T(8,128)(2,1)S(1)}) custom-call(s32[1]{0:T(128)} %bitcast.first_ref, s32[1]{0:T(128)} %bitcast.1.expert_ref, bf16[16,64,256]{2,1,0:T(8,128)(2,1)} %copy-done.1, bf16[16,64,256]{2,1,0:T(8,128)(2,1)} %copy-done.3, ...), custom_call_target="tpu_custom_call" | custom-call | tf_op jit(solution)/shard_map/pallas_call | solution.py:118
  132.0 0.0 collective-permute-done.7.refs_1_
  132.0 1.1 collective-permute-done.8.refs_2_
  133.1 3.7 %collective-permute-done.9.refs_3_ = bf16[16,32,256]{2,1,0:T(8,128)(2,1)S(1)} collective-permute-done((bf16[16,32,256]{2,1,0:T(8,128)(2,1)S(1)}, bf16[16,32,256]{2,1,0:T(8,128)(2,1)S(1)}, u32[]{:S(2)}, u32[]{:S(2)}) %collective-permute-start.9) | collective-permute-done | bytes 262176 | tf_op jit(solution)/shard_map/ppermute | solution.py:35
  136.8 1.3 shard_map.105
  138.1 2.0 %collective-permute-start.10 = (bf16[4,32,2048]{2,1,0:T(8,128)(2,1)S(1)}, bf16[4,32,2048]{2,1,0:T(8,128)(2,1)S(1)}, u32[]{:S(2)}, u32[]{:S(2)}) collective-permute-start(bf16[4,32,2048]{2,1,0:T(8,128)(2,1)S(1)} %get-tuple-element.15), channel_id=1, source_target_pairs={{0,4},{4,0},{1,5},{5,1},{2,6},{6,2},{3,7},{7,3},{8,12},{12,8},{9,1... | collective-permute-start | bytes 1572872 | tf_op jit(solution)/shard_map/ppermute | solution.py:39
  140.1 1.8 %collective-permute-done.10 = bf16[4,32,2048]{2,1,0:T(8,128)(2,1)S(1)} collective-permute-done((bf16[4,32,2048]{2,1,0:T(8,128)(2,1)S(1)}, bf16[4,32,2048]{2,1,0:T(8,128)(2,1)S(1)}, u32[]{:S(2)}, u32[]{:S(2)}) %collective-permute-start.10) | collective-permute-done | bytes 524320 | tf_op jit(solution)/shard_map/ppermute | solution.py:39
  141.9 0.1 add_convert_fusion
  142.0 12.5 %all_to_all.21 = bf16[4,32,2048]{2,1,0:T(8,128)(2,1)S(1)} all-to-all(bf16[4,32,2048]{2,1,0:T(8,128)(2,1)S(1)} %add_convert_fusion), channel_id=1, replica_groups=mesh['z'=16,'x'=4,'c'=2,'y'=4] {'x'}, dimensions={0} | all-to-all | bytes 1048576 | tf_op jit(solution)/shard_map/all_to_all | solution.py:206
  154.5 0.1 reduce_sum.44
  154.6 0.1 reshape.71
  154.7 23.0 %all_to_all.22 = bf16[16,2,2048]{2,1,0:T(2,128)(2,1)S(1)} all-to-all(bf16[16,2,2048]{2,1,0:T(2,128)(2,1)S(1)} %reshape.71), channel_id=1, replica_groups=mesh['z'=16,'x'=4,'c'=2,'y'=4] {'z'}, dimensions={0} | all-to-all | bytes 262144 | tf_op jit(solution)/shard_map/all_to_all | solution.py:208
  177.7 0.7 reduce_sum.45
  (10 shorter events, 0.2 us)
Async XLA Ops:
  3.0 9.3 %copy-start.5 = (bf16[2,2048]{1,0:T(2,128)(2,1)S(1)}, bf16[2,2048]{1,0:T(2,128)(2,1)}, u32[]{:S(2)}) copy-start(bf16[2,2048]{1,0:T(2,128)(2,1)} %param.7) | copy-start | bytes 24580
  3.0 9.8 %copy-start.6 = (s32[2,2]{1,0:T(2,128)S(1)}, s32[2,2]{1,0:T(2,128)}, u32[]{:S(2)}) copy-start(s32[2,2]{1,0:T(2,128)} %param.8) | copy-start | bytes 52
  3.0 9.9 %copy-start.7 = (f32[2,2]{1,0:T(2,128)S(1)}, f32[2,2]{1,0:T(2,128)}, u32[]{:S(2)}) copy-start(f32[2,2]{1,0:T(2,128)} %param.9) | copy-start | bytes 52
  3.0 21.9 %all-to-all-start = ((bf16[32,3,16,256]{3,2,1,0:T(8,128)(2,1)}), bf16[32,3,16,256]{3,2,1,0:T(8,128)(2,1)S(1)}, u32[]{:S(2)}, u32[]{:S(2)}) async-start(bf16[32,3,16,256]{3,2,1,0:T(8,128)(2,1)} %bitcast.5), calls=%async_computation | async-start | bytes 1572864 | tf_op jit(solution)/shard_map/all_to_all | solution.py:148
  87.6 16.1 %collective-permute-start.3 = (bf16[32,2176]{1,0:T(8,128)(2,1)S(1)}, bf16[32,2176]{1,0:T(8,128)(2,1)S(1)}, u32[]{:S(2)}, u32[]{:S(2)}) collective-permute-start(bf16[32,2176]{1,0:T(8,128)(2,1)S(1)} %pad_maximum_fusion.1), channel_id=1, source_target_pairs={{0,8},{8,16},{16,24},{24,0},{1,9},{9,17},{17,25},{25,1},{2,10},{10... | collective-permute-start | bytes 417800 | tf_op jit(solution)/shard_map/ppermute | solution.py:35
  90.2 13.5 %collective-permute-start.4 = (bf16[32,2176]{1,0:T(8,128)(2,1)S(1)}, bf16[32,2176]{1,0:T(8,128)(2,1)S(1)}, u32[]{:S(2)}, u32[]{:S(2)}) collective-permute-start(bf16[32,2176]{1,0:T(8,128)(2,1)S(1)} %pad_maximum_fusion.1), channel_id=1, source_target_pairs={{0,16},{8,24},{16,0},{24,8},{1,17},{9,25},{17,1},{25,9},{2,18},{10... | collective-permute-start | bytes 417800 | tf_op jit(solution)/shard_map/ppermute | solution.py:35
  93.9 9.8 %collective-permute-start.5 = (bf16[32,2176]{1,0:T(8,128)(2,1)S(1)}, bf16[32,2176]{1,0:T(8,128)(2,1)S(1)}, u32[]{:S(2)}, u32[]{:S(2)}) collective-permute-start(bf16[32,2176]{1,0:T(8,128)(2,1)S(1)} %pad_maximum_fusion.1), channel_id=1, source_target_pairs={{0,24},{8,0},{16,8},{24,16},{1,25},{9,1},{17,9},{25,17},{2,26},{10... | collective-permute-start | bytes 417800 | tf_op jit(solution)/shard_map/ppermute | solution.py:35
  96.7 30.9 %copy-start.1 = (bf16[16,64,256]{2,1,0:T(8,128)(2,1)}, bf16[16,64,256]{2,1,0:T(8,128)(2,1)S(1)}, u32[]{:S(2)}) copy-start(bf16[16,64,256]{2,1,0:T(8,128)(2,1)S(1)} %slice.34.refs_0_) | copy-start | bytes 1572868
  96.8 20.4 %collective-permute-start = (bf16[16,64,256]{2,1,0:T(8,128)(2,1)S(1)}, bf16[16,64,256]{2,1,0:T(8,128)(2,1)S(1)}, u32[]{:S(2)}, u32[]{:S(2)}) collective-permute-start(bf16[16,64,256]{2,1,0:T(8,128)(2,1)S(1)} %slice.34.refs_0_), channel_id=1, source_target_pairs={{0,1},{1,2},{2,3},{3,0},{4,5},{5,6},{6,7},{7,4},{8,9},{9,10},{10,1... | collective-permute-start | bytes 1572872 | tf_op jit(solution)/shard_map/ppermute | solution.py:35
  101.8 17.3 %collective-permute-start.1 = (bf16[16,64,256]{2,1,0:T(8,128)(2,1)S(1)}, bf16[16,64,256]{2,1,0:T(8,128)(2,1)S(1)}, u32[]{:S(2)}, u32[]{:S(2)}) collective-permute-start(bf16[16,64,256]{2,1,0:T(8,128)(2,1)S(1)} %slice.34.refs_0_), channel_id=1, source_target_pairs={{0,2},{1,3},{2,0},{3,1},{4,6},{5,7},{6,4},{7,5},{8,10},{9,11},{10,... | collective-permute-start | bytes 1572872 | tf_op jit(solution)/shard_map/ppermute | solution.py:35
  103.8 23.8 %copy-start = (bf16[128,2176]{1,0:T(8,128)(2,1)}, bf16[128,2176]{1,0:T(8,128)(2,1)S(1)}, u32[]{:S(2)}) copy-start(bf16[128,2176]{1,0:T(8,128)(2,1)S(1)} %pad_maximum_fusion.refs_4_) | copy-start | bytes 1671172
  103.8 23.8 %collective-permute-start.6 = (bf16[128,2176]{1,0:T(8,128)(2,1)S(1)}, bf16[128,2176]{1,0:T(8,128)(2,1)S(1)}, u32[]{:S(2)}, u32[]{:S(2)}) collective-permute-start(bf16[128,2176]{1,0:T(8,128)(2,1)S(1)} %pad_maximum_fusion.refs_4_), channel_id=1, source_target_pairs={{0,4},{4,0},{1,5},{5,1},{2,6},{6,2},{3,7},{7,3},{8,12},{12,8},{9,1... | collective-permute-start | bytes 1671176 | tf_op jit(solution)/shard_map/ppermute | solution.py:39
  105.7 21.9 %collective-permute-start.2 = (bf16[16,64,256]{2,1,0:T(8,128)(2,1)S(1)}, bf16[16,64,256]{2,1,0:T(8,128)(2,1)}, u32[]{:S(2)}, u32[]{:S(2)}) collective-permute-start(bf16[16,64,256]{2,1,0:T(8,128)(2,1)S(1)} %slice.34.refs_0_), channel_id=1, source_target_pairs={{0,3},{1,0},{2,1},{3,2},{4,7},{5,4},{6,5},{7,6},{8,11},{9,8},{10,9... | collective-permute-start | bytes 1572872 | tf_op jit(solution)/shard_map/ppermute | solution.py:35
  108.9 23.1 %collective-permute-start.7 = (bf16[16,32,256]{2,1,0:T(8,128)(2,1)S(1)}, bf16[16,32,256]{2,1,0:T(8,128)(2,1)S(1)}, u32[]{:S(2)}, u32[]{:S(2)}) collective-permute-start(bf16[16,32,256]{2,1,0:T(8,128)(2,1)S(1)} %slice.37.refs_0_), channel_id=1, source_target_pairs={{0,1},{1,2},{2,3},{3,0},{4,5},{5,6},{6,7},{7,4},{8,9},{9,10},{10,1... | collective-permute-start | bytes 786440 | tf_op jit(solution)/shard_map/ppermute | solution.py:35
  117.2 10.5 %copy-start.3 = (bf16[16,64,256]{2,1,0:T(8,128)(2,1)}, bf16[16,64,256]{2,1,0:T(8,128)(2,1)S(1)}, u32[]{:S(2)}) copy-start(bf16[16,64,256]{2,1,0:T(8,128)(2,1)S(1)} %collective-permute-done.refs_1_) | copy-start | bytes 1572868
  117.2 15.9 %collective-permute-start.8 = (bf16[16,32,256]{2,1,0:T(8,128)(2,1)S(1)}, bf16[16,32,256]{2,1,0:T(8,128)(2,1)S(1)}, u32[]{:S(2)}, u32[]{:S(2)}) collective-permute-start(bf16[16,32,256]{2,1,0:T(8,128)(2,1)S(1)} %slice.37.refs_0_), channel_id=1, source_target_pairs={{0,2},{1,3},{2,0},{3,1},{4,6},{5,7},{6,4},{7,5},{8,10},{9,11},{10,... | collective-permute-start | bytes 786440 | tf_op jit(solution)/shard_map/ppermute | solution.py:35
  119.1 0.8 copy-start.4
  119.9 16.9 %collective-permute-start.9 = (bf16[16,32,256]{2,1,0:T(8,128)(2,1)S(1)}, bf16[16,32,256]{2,1,0:T(8,128)(2,1)S(1)}, u32[]{:S(2)}, u32[]{:S(2)}) collective-permute-start(bf16[16,32,256]{2,1,0:T(8,128)(2,1)S(1)} %slice.37.refs_0_), channel_id=1, source_target_pairs={{0,3},{1,0},{2,1},{3,2},{4,7},{5,4},{6,5},{7,6},{8,11},{9,8},{10,9... | collective-permute-start | bytes 786440 | tf_op jit(solution)/shard_map/ppermute | solution.py:35
  127.6 0.8 copy-start.2
  138.1 3.8 %collective-permute-start.10 = (bf16[4,32,2048]{2,1,0:T(8,128)(2,1)S(1)}, bf16[4,32,2048]{2,1,0:T(8,128)(2,1)S(1)}, u32[]{:S(2)}, u32[]{:S(2)}) collective-permute-start(bf16[4,32,2048]{2,1,0:T(8,128)(2,1)S(1)} %get-tuple-element.15), channel_id=1, source_target_pairs={{0,4},{4,0},{1,5},{5,1},{2,6},{6,2},{3,7},{7,3},{8,12},{12,8},{9,1... | collective-permute-start | bytes 1572872 | tf_op jit(solution)/shard_map/ppermute | solution.py:39

commit v2 on v1

--- a/solution.py
+++ b/solution.py
@@ -11,6 +11,7 @@
 FS_TP = ("z", "x", "c", "y")
 NZ, NX, NC, NY = 16, 4, 2, 4
 XC = NX * NC
+LANES = 128
 PAD = 128
 
 
@@ -56,24 +57,28 @@
 
 
 def sort_kernel(y_ref, swapped, riders, out):
-    kinds, depth = swapped.shape[2:4]
+    kinds, depth, wide = swapped.shape[2:]
     for e in range(NZ // NY):
         x = lax.rem(NX + e - y_ref[0], NX)
         for y in range(NY):
             at = 0
             for m in range(kinds):
-                for c in range(NC):
-                    out[NY * e + y, at : at + depth] = swapped[NC * x + c, y, m]
-                    at += depth
+                for lane in range(0, wide, LANES):
+                    for c in range(NC):
+                        part = swapped[NC * x + c, y, m, :, lane : lane + LANES]
+                        out[NY * e + y, at : at + depth] = part
+                        at += depth
             out[NY * e + y, at:] = riders[...]
 
 
 def put(first_ref, ins, outs):
     for k, part in enumerate(ins):
-        at = lax.rem(first_ref[0] + k, NX)
-        for m, out in enumerate(outs):
-            span = out.shape[2]
-            out[:, at] = part[:, m * span : (m + 1) * span]
+        at, row = lax.rem(first_ref[0] + k, NX), 0
+        for out in outs:
+            span, wide = out.shape[2:]
+            for lane in range(0, wide, LANES):
+                out[:, at, :, lane : lane + LANES] = part[:, row : row + span]
+                row += span
 
 
 def all_from(own, axis, size):
@@ -84,11 +89,8 @@
 
 
 def hidden_kernel(first_ref, expert_ref, *refs):
-    parts, (here, there, gate, up, out, rows) = refs[:NY], refs[NY:]
+    parts, (rows, gate, up, out) = refs[:NY], refs[NY:]
     put(first_ref, parts, (gate, up))
-    half = here.shape[0]
-    rows[:half] = here[...]
-    rows[half:] = there[...]
     width = gate.shape[0] * gate.shape[1] * gate.shape[2]
     table = rows[:, width:].astype(jnp.float32)
     lane = lax.broadcasted_iota(jnp.int32, table.shape, 1)
@@ -96,21 +98,19 @@
     x = rows[:, :width]
     g = jnp.dot(x, gate[...].reshape(width, -1), preferred_element_type=jnp.float32)
     u = jnp.dot(x, up[...].reshape(width, -1), preferred_element_type=jnp.float32)
-    out[...] = (weight * (g / (1.0 + jnp.exp(-g))) * u).astype(jnp.bfloat16)
-
-
-def down_kernel(first_ref, x_ref, *refs):
+    hidden = (weight * (g / (1.0 + jnp.exp(-g))) * u).astype(jnp.bfloat16)
+    out[...] = hidden.reshape(out.shape)
+
+
+def down_kernel(first_ref, c_ref, *refs):
     parts, (hidden, down, theirs, mine) = refs[:NY], refs[NY:]
     put(first_ref, parts, (down,))
     full = down[...].reshape(-1, down.shape[3])
-    half = hidden.shape[0] // 2
     dims = (((1,), (1,)), ((), ()))
-    both = lax.dot_general(hidden[...], full, dims, preferred_element_type=jnp.float32)
-    both = both.reshape(2, NX, half // NX, both.shape[1])
-    for k in range(NX):
-        to = lax.rem(NX + x_ref[0] - k, NX)
-        mine[to] = both[0, k]
-        theirs[to] = both[1, k].astype(jnp.bfloat16)
+    for out, core in ((theirs, 1 - c_ref[0]), (mine, c_ref[0])):
+        act = hidden[:, core].reshape(-1, full.shape[1])
+        got = lax.dot_general(act, full, dims, preferred_element_type=jnp.float32)
+        out[...] = got.reshape(out.shape).astype(out.dtype)
 
 
 def on_core(kernel, scalars, arrays, outs, scratch=(), limit=None):
@@ -133,10 +133,10 @@
     experts, depth, wide = gate_train.shape
     own_rows, width = tokens.shape
     block = wide // XC
-    y, x = lax.axis_index("y"), lax.axis_index("x")
+    y, x, c = (lax.axis_index(axis) for axis in ("y", "x", "c"))
     expert = lax.axis_index("z") // (NZ // experts)
     first_block = lax.rem(NX + expert - y, NX).reshape(1).astype(jnp.int32)
-    expert, y, x = (i.reshape(1).astype(jnp.int32) for i in (expert, y, x))
+    expert, y, x, c = (i.reshape(1).astype(jnp.int32) for i in (expert, y, x, c))
 
     bf16, f32 = jnp.bfloat16, jnp.float32
     (local,) = on_core(
@@ -151,50 +151,51 @@
 
     normed = normalize(tokens)
     table = route_table(route_experts, route_logits, experts)
-    spread = own_rows * width // block
+    spread = own_rows * width // LANES
     riders = jnp.concatenate(
         [
-            normed.reshape(spread, block),
-            jnp.pad(table, ((0, 8 - own_rows), (0, block - experts))),
+            normed.reshape(spread, LANES),
+            jnp.pad(table, ((0, 8 - own_rows), (0, LANES - experts))),
         ]
     )
     span = NC * depth
-    cut = 3 * span
+    one = span * (block // LANES)
+    cut = 3 * one
     (sorted_by_z,) = on_core(
         sort_kernel,
         (y,),
         (held(swapped.reshape(XC, NY, 3, depth, block)), held(riders)),
-        [pltpu.VMEM((NZ, cut + spread + 8, block), bf16)],
+        [pltpu.VMEM((NZ, cut + spread + 8, LANES), bf16)],
         limit=8 << 20,
     )
     first = lax.all_to_all(sorted_by_z, "z", 0, 0, tiled=True)
 
-    parts = all_from(first[:, : 2 * span], "y", NY)
+    parts = all_from(first[:, : 2 * one], "y", NY)
     rows_z = first[:, cut : cut + spread].reshape(NZ * own_rows, width)
-    table_z = first[:, cut + spread : cut + spread + own_rows, :PAD]
+    table_z = first[:, cut + spread : cut + spread + own_rows]
     rows_z = jnp.concatenate([rows_z, table_z.reshape(NZ * own_rows, PAD)], axis=1)
-    rows_x = all_from(rows_z, "x", NX)
-    rows_x = jnp.concatenate(rows_x)
-    rows_c = swap_core(rows_x)
+    copies = jnp.broadcast_to(rows_z[None], (XC, *rows_z.shape))
+    rows_all = lax.all_to_all(copies, ("x", "c"), 0, 0, tiled=True)
+    rows_all = rows_all.reshape(-1, width + PAD)
     placed = jax.ShapeDtypeStruct((NZ, NX, span, block), bf16)
-    half = rows_x.shape[0]
+    count = rows_all.shape[0]
     gate_serve, up_serve, hidden = on_core(
         hidden_kernel,
         (first_block, expert),
-        (*parts, rows_x, rows_c),
-        [placed, placed, pltpu.VMEM((2 * half, block), bf16)],
-        [pltpu.VMEM((2 * half, width + PAD), bf16)],
-    )
-
-    parts = all_from(first[:, 2 * span : cut], "y", NY)
+        [held(a) for a in (*parts, rows_all)],
+        [placed, placed, pltpu.VMEM((NX, NC, count // XC, block), bf16)],
+        limit=16 << 20,
+    )
+
+    parts = all_from(first[:, 2 * one : cut], "y", NY)
     down_serve, theirs, mine = on_core(
         down_kernel,
-        (first_block, x),
+        (first_block, c),
         [held(a) for a in (*parts, hidden)],
         [
             placed,
-            pltpu.VMEM((NX, half // NX, width), bf16),
-            pltpu.VMEM((NX, half // NX, width), f32),
+            pltpu.VMEM((NX, count // XC, width), bf16),
+            pltpu.VMEM((NX, count // XC, width), f32),
         ],
         limit=16 << 20,
     )

time: 179 us -> 176 us (0.983)
  waiting for transfers between devices: 23.4 us -> 35.5 us
  starting transfers between devices: 45.1 us -> 33.2 us
  blocking collectives: 97.9 us -> 94.6 us
    ppermute x9 -> x6, starting transfers between devices: 31.9 us -> 18.5 us  [shift(): lax.ppermute(array, axis, [(i, (i + by) % size) for i in range(size)])]
    ppermute x9 -> x6, waiting for transfers between devices: 9.92 us -> 22 us  [shift(): lax.ppermute(array, axis, [(i, (i + by) % size) for i in range(size)])]
    all_to_all x0 -> x1, starting transfers between devices: none -> 3.56 us  [per_device(): rows_all = lax.all_to_all(copies, ('x', 'c'), 0, 0, tiled=True)]
    all_to_all x1, blocking collectives: 23 us -> 19.7 us  [per_device(): lax.all_to_all(by_x, 'z', 0, 0, tiled=True).astype(jnp.float32).sum(axis=0)]
    ppermute x2 -> x1, starting transfers between devices: 3.89 us -> 1.91 us  [swap_core(): return lax.ppermute(array, 'c', [(0, 1), (1, 0)])]
  transfers between devices with their start and end apart: 12 -> 9, of which waited for: 6 -> 6; matrix products, arithmetic and copies ran while one was open for 1% -> 1% of each run, Pallas kernels for 2% -> 1%
where the time goes in v2:
time: 176 us; the launch traced here: 175 us
  blocking collectives  94.6 us (54%)
  waiting for transfers between devices  35.5 us (20%)
  starting transfers between devices  33.2 us (19%)
  Pallas kernels  6.86 us (4%)
  local copies, waits for them, and re-layouts  2.59 us (1%)
    all_to_all x1, blocking collectives, per_device(): first = lax.all_to_all(sorted_by_z, 'z', 0, 0, tiled=True)  60.9 us
    ppermute x6, waiting for transfers between devices, shift(): lax.ppermute(array, axis, [(i, (i + by) % size) for i in range(size)])  22 us
    all_to_all x1, blocking collectives, per_device(): lax.all_to_all(by_x, 'z', 0, 0, tiled=True).astype(jnp.float32).sum(axis=0)  19.7 us
    ppermute x6, starting transfers between devices, shift(): lax.ppermute(array, axis, [(i, (i + by) % size) for i in range(size)])  18.5 us
    all_to_all x1, blocking collectives, per_device(): lax.all_to_all(chip, 'x', 0, 0, tiled=True).astype(jnp.float32).sum(axis=0)  14 us
    all_to_all x1, waiting for transfers between devices, per_device(): lax.all_to_all(local.reshape(XC * NY, 3, depth, block), ('x', 'c', 'y'),...  11.6 us
    all_to_all x1, starting transfers between devices, per_device(): lax.all_to_all(local.reshape(XC * NY, 3, depth, block), ('x', 'c', 'y'),...  9.28 us
    pallas_call x4, Pallas kernels, on_core(): pl.pallas_call(kernel, out_shape=outs, in_specs=[smem] * len(scalars) + [...  6.86 us
  transfers between devices with their start and end apart: 9, of which 6 were waited for; matrix products, arithmetic and copies ran while one was open for 1% of the time, Pallas kernels for 1%

profile of v2, /device:TPU:24, one launch (start us, length us, event | category | flops | bytes accessed | tf_op | source)
XLA Modules:
  0.0 175.2 jit_solution(10332477737223335193)
XLA Ops:
  0.6 2.4 %shard_map.102 = bf16[8,4,3,16,256]{4,3,2,1,0:T(8,128)(2,1)} custom-call(s32[1]{0:T(128)} %bitcast.3.x_ref, f32[1,16]{1,0:T(1,128)} %bitcast.16, f32[4,16,2048]{2,1,0:T(8,128)} %gate.1, f32[4,16,2048]{2,1,0:T(8,128)} %up.1, f32[4,16,2048]{2,1,0:T(8,128)} %down.1), custom_call_target="tpu_custom_call" | custom-call | tf_op jit(solution)/shard_map/pallas_call | solution.py:118
  3.0 0.0 copy-start.1
  3.0 0.0 copy-start.2
  3.0 0.0 copy-start.3
  3.0 9.3 %all-to-all-start = ((bf16[32,3,16,256]{3,2,1,0:T(8,128)(2,1)}), bf16[32,3,16,256]{3,2,1,0:T(8,128)(2,1)S(1)}, u32[]{:S(2)}, u32[]{:S(2)}) async-start(bf16[32,3,16,256]{3,2,1,0:T(8,128)(2,1)} %bitcast.5), calls=%async_computation | async-start | bytes 1572864 | tf_op jit(solution)/shard_map/all_to_all | solution.py:148
  12.3 0.0 copy-done.1
  12.3 0.1 convert_reduce_fusion
  12.5 0.2 fusion.3
  12.7 0.1 fusion.4
  12.8 0.0 copy-done.2
  12.8 0.2 slice_reduce_fusion.1
  13.0 0.0 copy-done.3
  13.0 0.2 fusion.8
  13.2 0.1 fusion.7
  13.3 11.6 %all-to-all-done = bf16[32,3,16,256]{3,2,1,0:T(8,128)(2,1)S(1)} async-done(((bf16[32,3,16,256]{3,2,1,0:T(8,128)(2,1)}), bf16[32,3,16,256]{3,2,1,0:T(8,128)(2,1)S(1)}, u32[]{:S(2)}, u32[]{:S(2)}) %all-to-all-start) | async-done | bytes 786464 | tf_op jit(solution)/shard_map/all_to_all | solution.py:148
  24.9 0.2 shard_map.103
  25.1 60.9 %all_to_all.25 = bf16[16,232,128]{2,1,0:T(8,128)(2,1)S(1)} all-to-all(bf16[16,232,128]{2,1,0:T(8,128)(2,1)S(1)} %shard_map.103), channel_id=1, replica_groups=mesh['z'=16,'x'=4,'c'=2,'y'=4] {'z'}, dimensions={0} | all-to-all | bytes 1900544 | tf_op jit(solution)/shard_map/all_to_all | solution.py:171
  85.9 0.0 copy-start
  86.0 0.1 reshape.73
  86.1 1.2 broadcast_in_dim.5
  87.2 3.6 %all-to-all-start.2 = ((bf16[8,32,2176]{2,1,0:T(8,128)(2,1)}), bf16[8,32,2176]{2,1,0:T(8,128)(2,1)S(1)}, u32[]{:S(2)}, u32[]{:S(2)}) async-start(bf16[8,32,2176]{2,1,0:T(8,128)(2,1)} %broadcast_in_dim.5), calls=%async_computation.2 | async-start | bytes 2228224 | tf_op jit(solution)/shard_map/all_to_all | solution.py:178
  90.8 0.0 copy-done
  90.9 3.4 %collective-permute-start = (bf16[16,128,128]{2,1,0:T(8,128)(2,1)S(1)}, bf16[16,128,128]{2,1,0:T(8,128)(2,1)S(1)}, u32[]{:S(2)}, u32[]{:S(2)}) collective-permute-start(bf16[16,128,128]{2,1,0:T(8,128)(2,1)S(1)} %slice.34.refs_0_), channel_id=1, source_target_pairs={{0,1},{1,2},{2,3},{3,0},{4,5},{5,6},{6,7},{7,4},{8,9},{9,10},{10,1... | collective-permute-start | bytes 1572872 | tf_op jit(solution)/shard_map/ppermute | solution.py:36
  94.3 3.0 %collective-permute-start.1 = (bf16[16,128,128]{2,1,0:T(8,128)(2,1)S(1)}, bf16[16,128,128]{2,1,0:T(8,128)(2,1)S(1)}, u32[]{:S(2)}, u32[]{:S(2)}) collective-permute-start(bf16[16,128,128]{2,1,0:T(8,128)(2,1)S(1)} %slice.34.refs_0_), channel_id=1, source_target_pairs={{0,2},{1,3},{2,0},{3,1},{4,6},{5,7},{6,4},{7,5},{8,10},{9,11},{10,... | collective-permute-start | bytes 1572872 | tf_op jit(solution)/shard_map/ppermute | solution.py:36
  97.2 2.8 %collective-permute-start.2 = (bf16[16,128,128]{2,1,0:T(8,128)(2,1)S(1)}, bf16[16,128,128]{2,1,0:T(8,128)(2,1)S(1)}, u32[]{:S(2)}, u32[]{:S(2)}) collective-permute-start(bf16[16,128,128]{2,1,0:T(8,128)(2,1)S(1)} %slice.34.refs_0_), channel_id=1, source_target_pairs={{0,3},{1,0},{2,1},{3,2},{4,7},{5,4},{6,5},{7,6},{8,11},{9,8},{10,9... | collective-permute-start | bytes 1572872 | tf_op jit(solution)/shard_map/ppermute | solution.py:36
  100.1 1.0 slice.37.refs_0_
  101.1 4.2 %collective-permute-start.3 = (bf16[16,64,128]{2,1,0:T(8,128)(2,1)S(1)}, bf16[16,64,128]{2,1,0:T(8,128)(2,1)}, u32[]{:S(2)}, u32[]{:S(2)}) collective-permute-start(bf16[16,64,128]{2,1,0:T(8,128)(2,1)S(1)} %slice.37.refs_0_), channel_id=1, source_target_pairs={{0,1},{1,2},{2,3},{3,0},{4,5},{5,6},{6,7},{7,4},{8,9},{9,10},{10,1... | collective-permute-start | bytes 786440 | tf_op jit(solution)/shard_map/ppermute | solution.py:36
  105.3 3.2 %collective-permute-start.4 = (bf16[16,64,128]{2,1,0:T(8,128)(2,1)S(1)}, bf16[16,64,128]{2,1,0:T(8,128)(2,1)}, u32[]{:S(2)}, u32[]{:S(2)}) collective-permute-start(bf16[16,64,128]{2,1,0:T(8,128)(2,1)S(1)} %slice.37.refs_0_), channel_id=1, source_target_pairs={{0,2},{1,3},{2,0},{3,1},{4,6},{5,7},{6,4},{7,5},{8,10},{9,11},{10,... | collective-permute-start | bytes 786440 | tf_op jit(solution)/shard_map/ppermute | solution.py:36
  108.5 8.8 %collective-permute-done.refs_1_ = bf16[16,128,128]{2,1,0:T(8,128)(2,1)S(1)} collective-permute-done((bf16[16,128,128]{2,1,0:T(8,128)(2,1)S(1)}, bf16[16,128,128]{2,1,0:T(8,128)(2,1)S(1)}, u32[]{:S(2)}, u32[]{:S(2)}) %collective-permute-start) | collective-permute-done | bytes 524320 | tf_op jit(solution)/shard_map/ppermute | solution.py:36
  117.2 1.9 %collective-permute-start.5 = (bf16[16,64,128]{2,1,0:T(8,128)(2,1)S(1)}, bf16[16,64,128]{2,1,0:T(8,128)(2,1)}, u32[]{:S(2)}, u32[]{:S(2)}) collective-permute-start(bf16[16,64,128]{2,1,0:T(8,128)(2,1)S(1)} %slice.37.refs_0_), channel_id=1, source_target_pairs={{0,3},{1,0},{2,1},{3,2},{4,7},{5,4},{6,5},{7,6},{8,11},{9,8},{10,9... | collective-permute-start | bytes 786440 | tf_op jit(solution)/shard_map/ppermute | solution.py:36
  119.2 0.0 collective-permute-done.1.refs_2_
  119.2 4.6 %collective-permute-done.2.refs_3_ = bf16[16,128,128]{2,1,0:T(8,128)(2,1)S(1)} collective-permute-done((bf16[16,128,128]{2,1,0:T(8,128)(2,1)S(1)}, bf16[16,128,128]{2,1,0:T(8,128)(2,1)S(1)}, u32[]{:S(2)}, u32[]{:S(2)}) %collective-permute-start.2) | collective-permute-done | bytes 524320 | tf_op jit(solution)/shard_map/ppermute | solution.py:36
  123.8 0.0 all-to-all-done.2
  123.8 1.9 %shard_map.104 = (bf16[16,4,32,256]{3,2,1,0:T(8,128)(2,1)}, bf16[16,4,32,256]{3,2,1,0:T(8,128)(2,1)}, bf16[4,2,32,256]{3,2,1,0:T(8,128)(2,1)S(1)}) custom-call(s32[1]{0:T(128)} %bitcast.first_ref, s32[1]{0:T(128)} %bitcast.1.expert_ref, bf16[16,128,128]{2,1,0:T(8,128)(2,1)S(1)} %slice.34.refs_0_, bf16[16,128,128]{2,1,0:T(8,128)(2,1)S(1)} %collective-permute-done.refs_1_, ...), custom_call_target="tpu_custom_call" | custom-call | tf_op jit(solution)/shard_map/pallas_call | solution.py:118
  125.7 0.0 collective-permute-done.3.refs_1_
  125.7 3.8 %collective-permute-done.4.refs_2_ = bf16[16,64,128]{2,1,0:T(8,128)(2,1)} collective-permute-done((bf16[16,64,128]{2,1,0:T(8,128)(2,1)S(1)}, bf16[16,64,128]{2,1,0:T(8,128)(2,1)}, u32[]{:S(2)}, u32[]{:S(2)}) %collective-permute-start.4) | collective-permute-done | bytes 262176 | tf_op jit(solution)/shard_map/ppermute | solution.py:36
  129.5 4.8 %collective-permute-done.5.refs_3_ = bf16[16,64,128]{2,1,0:T(8,128)(2,1)} collective-permute-done((bf16[16,64,128]{2,1,0:T(8,128)(2,1)S(1)}, bf16[16,64,128]{2,1,0:T(8,128)(2,1)}, u32[]{:S(2)}, u32[]{:S(2)}) %collective-permute-start.5) | collective-permute-done | bytes 262176 | tf_op jit(solution)/shard_map/ppermute | solution.py:36
  134.3 2.4 %shard_map.105 = (bf16[16,4,32,256]{3,2,1,0:T(8,128)(2,1)}, bf16[4,32,2048]{2,1,0:T(8,128)(2,1)S(1)}, f32[4,32,2048]{2,1,0:T(8,128)S(1)}) custom-call(s32[1]{0:T(128)} %bitcast.first_ref, s32[1]{0:T(128)} %bitcast.11.c_ref, bf16[16,64,128]{2,1,0:T(8,128)(2,1)S(1)} %slice.37.refs_0_, bf16[16,64,128]{2,1,0:T(8,128)(2,1)} %collective-permute-done.3.refs_1_, ...), custom_call_target="tpu_custom_call" | custom-call | tf_op jit(solution)/shard_map/pallas_call | solution.py:118
  136.7 1.9 %collective-permute-start.6 = (bf16[4,32,2048]{2,1,0:T(8,128)(2,1)S(1)}, bf16[4,32,2048]{2,1,0:T(8,128)(2,1)S(1)}, u32[]{:S(2)}, u32[]{:S(2)}) collective-permute-start(bf16[4,32,2048]{2,1,0:T(8,128)(2,1)S(1)} %get-tuple-element.15), channel_id=1, source_target_pairs={{0,4},{4,0},{1,5},{5,1},{2,6},{6,2},{3,7},{7,3},{8,12},{12,8},{9,1... | collective-permute-start | bytes 1572872 | tf_op jit(solution)/shard_map/ppermute | solution.py:40
  138.6 1.9 %collective-permute-done.6 = bf16[4,32,2048]{2,1,0:T(8,128)(2,1)S(1)} collective-permute-done((bf16[4,32,2048]{2,1,0:T(8,128)(2,1)S(1)}, bf16[4,32,2048]{2,1,0:T(8,128)(2,1)S(1)}, u32[]{:S(2)}, u32[]{:S(2)}) %collective-permute-start.6) | collective-permute-done | bytes 524320 | tf_op jit(solution)/shard_map/ppermute | solution.py:40
  140.5 0.1 add_convert_fusion
  140.6 14.0 %all_to_all.26 = bf16[4,32,2048]{2,1,0:T(8,128)(2,1)S(1)} all-to-all(bf16[4,32,2048]{2,1,0:T(8,128)(2,1)S(1)} %add_convert_fusion), channel_id=1, replica_groups=mesh['z'=16,'x'=4,'c'=2,'y'=4] {'x'}, dimensions={0} | all-to-all | bytes 1048576 | tf_op jit(solution)/shard_map/all_to_all | solution.py:207
  154.6 0.1 reduce_sum.44
  154.7 0.1 reshape.80
  154.8 19.7 %all_to_all.27 = bf16[16,2,2048]{2,1,0:T(2,128)(2,1)S(1)} all-to-all(bf16[16,2,2048]{2,1,0:T(2,128)(2,1)S(1)} %reshape.80), channel_id=1, replica_groups=mesh['z'=16,'x'=4,'c'=2,'y'=4] {'z'}, dimensions={0} | all-to-all | bytes 262144 | tf_op jit(solution)/shard_map/all_to_all | solution.py:209
  174.5 0.7 reduce_sum.45
  (8 shorter events, 0.1 us)
Async XLA Ops:
  3.0 9.3 %copy-start.1 = (bf16[2,2048]{1,0:T(2,128)(2,1)S(1)}, bf16[2,2048]{1,0:T(2,128)(2,1)}, u32[]{:S(2)}) copy-start(bf16[2,2048]{1,0:T(2,128)(2,1)} %param.7) | copy-start | bytes 24580
  3.0 9.8 %copy-start.2 = (s32[2,2]{1,0:T(2,128)S(1)}, s32[2,2]{1,0:T(2,128)}, u32[]{:S(2)}) copy-start(s32[2,2]{1,0:T(2,128)} %param.8) | copy-start | bytes 52
  3.0 9.9 %copy-start.3 = (f32[2,2]{1,0:T(2,128)S(1)}, f32[2,2]{1,0:T(2,128)}, u32[]{:S(2)}) copy-start(f32[2,2]{1,0:T(2,128)} %param.9) | copy-start | bytes 52
  3.0 21.9 %all-to-all-start = ((bf16[32,3,16,256]{3,2,1,0:T(8,128)(2,1)}), bf16[32,3,16,256]{3,2,1,0:T(8,128)(2,1)S(1)}, u32[]{:S(2)}, u32[]{:S(2)}) async-start(bf16[32,3,16,256]{3,2,1,0:T(8,128)(2,1)} %bitcast.5), calls=%async_computation | async-start | bytes 1572864 | tf_op jit(solution)/shard_map/all_to_all | solution.py:148
  85.9 4.9 %copy-start = (bf16[16,232,128]{2,1,0:T(8,128)(2,1)}, bf16[16,232,128]{2,1,0:T(8,128)(2,1)S(1)}, u32[]{:S(2)}) copy-start(bf16[16,232,128]{2,1,0:T(8,128)(2,1)S(1)} %all_to_all.25) | copy-start | bytes 2850820
  87.2 36.6 %all-to-all-start.2 = ((bf16[8,32,2176]{2,1,0:T(8,128)(2,1)}), bf16[8,32,2176]{2,1,0:T(8,128)(2,1)S(1)}, u32[]{:S(2)}, u32[]{:S(2)}) async-start(bf16[8,32,2176]{2,1,0:T(8,128)(2,1)} %broadcast_in_dim.5), calls=%async_computation.2 | async-start | bytes 2228224 | tf_op jit(solution)/shard_map/all_to_all | solution.py:178
  90.9 26.4 %collective-permute-start = (bf16[16,128,128]{2,1,0:T(8,128)(2,1)S(1)}, bf16[16,128,128]{2,1,0:T(8,128)(2,1)S(1)}, u32[]{:S(2)}, u32[]{:S(2)}) collective-permute-start(bf16[16,128,128]{2,1,0:T(8,128)(2,1)S(1)} %slice.34.refs_0_), channel_id=1, source_target_pairs={{0,1},{1,2},{2,3},{3,0},{4,5},{5,6},{6,7},{7,4},{8,9},{9,10},{10,1... | collective-permute-start | bytes 1572872 | tf_op jit(solution)/shard_map/ppermute | solution.py:36
  94.3 24.9 %collective-permute-start.1 = (bf16[16,128,128]{2,1,0:T(8,128)(2,1)S(1)}, bf16[16,128,128]{2,1,0:T(8,128)(2,1)S(1)}, u32[]{:S(2)}, u32[]{:S(2)}) collective-permute-start(bf16[16,128,128]{2,1,0:T(8,128)(2,1)S(1)} %slice.34.refs_0_), channel_id=1, source_target_pairs={{0,2},{1,3},{2,0},{3,1},{4,6},{5,7},{6,4},{7,5},{8,10},{9,11},{10,... | collective-permute-start | bytes 1572872 | tf_op jit(solution)/shard_map/ppermute | solution.py:36
  97.2 26.6 %collective-permute-start.2 = (bf16[16,128,128]{2,1,0:T(8,128)(2,1)S(1)}, bf16[16,128,128]{2,1,0:T(8,128)(2,1)S(1)}, u32[]{:S(2)}, u32[]{:S(2)}) collective-permute-start(bf16[16,128,128]{2,1,0:T(8,128)(2,1)S(1)} %slice.34.refs_0_), channel_id=1, source_target_pairs={{0,3},{1,0},{2,1},{3,2},{4,7},{5,4},{6,5},{7,6},{8,11},{9,8},{10,9... | collective-permute-start | bytes 1572872 | tf_op jit(solution)/shard_map/ppermute | solution.py:36
  101.1 24.6 %collective-permute-start.3 = (bf16[16,64,128]{2,1,0:T(8,128)(2,1)S(1)}, bf16[16,64,128]{2,1,0:T(8,128)(2,1)}, u32[]{:S(2)}, u32[]{:S(2)}) collective-permute-start(bf16[16,64,128]{2,1,0:T(8,128)(2,1)S(1)} %slice.37.refs_0_), channel_id=1, source_target_pairs={{0,1},{1,2},{2,3},{3,0},{4,5},{5,6},{6,7},{7,4},{8,9},{9,10},{10,1... | collective-permute-start | bytes 786440 | tf_op jit(solution)/shard_map/ppermute | solution.py:36
  105.3 24.2 %collective-permute-start.4 = (bf16[16,64,128]{2,1,0:T(8,128)(2,1)S(1)}, bf16[16,64,128]{2,1,0:T(8,128)(2,1)}, u32[]{:S(2)}, u32[]{:S(2)}) collective-permute-start(bf16[16,64,128]{2,1,0:T(8,128)(2,1)S(1)} %slice.37.refs_0_), channel_id=1, source_target_pairs={{0,2},{1,3},{2,0},{3,1},{4,6},{5,7},{6,4},{7,5},{8,10},{9,11},{10,... | collective-permute-start | bytes 786440 | tf_op jit(solution)/shard_map/ppermute | solution.py:36
  117.2 17.0 %collective-permute-start.5 = (bf16[16,64,128]{2,1,0:T(8,128)(2,1)S(1)}, bf16[16,64,128]{2,1,0:T(8,128)(2,1)}, u32[]{:S(2)}, u32[]{:S(2)}) collective-permute-start(bf16[16,64,128]{2,1,0:T(8,128)(2,1)S(1)} %slice.37.refs_0_), channel_id=1, source_target_pairs={{0,3},{1,0},{2,1},{3,2},{4,7},{5,4},{6,5},{7,6},{8,11},{9,8},{10,9... | collective-permute-start | bytes 786440 | tf_op jit(solution)/shard_map/ppermute | solution.py:36
  136.7 3.8 %collective-permute-start.6 = (bf16[4,32,2048]{2,1,0:T(8,128)(2,1)S(1)}, bf16[4,32,2048]{2,1,0:T(8,128)(2,1)S(1)}, u32[]{:S(2)}, u32[]{:S(2)}) collective-permute-start(bf16[4,32,2048]{2,1,0:T(8,128)(2,1)S(1)} %get-tuple-element.15), channel_id=1, source_target_pairs={{0,4},{4,0},{1,5},{5,1},{2,6},{6,2},{3,7},{7,3},{8,12},{12,8},{9,1... | collective-permute-start | bytes 1572872 | tf_op jit(solution)/shard_map/ppermute | solution.py:40

commit v3 on v2

--- a/solution.py
+++ b/solution.py
@@ -76,9 +76,9 @@
         at, row = lax.rem(first_ref[0] + k, NX), 0
         for out in outs:
             span, wide = out.shape[2:]
-            for lane in range(0, wide, LANES):
-                out[:, at, :, lane : lane + LANES] = part[:, row : row + span]
-                row += span
+            cuts = range(row, row + span * (wide // LANES), span)
+            out[:, at] = jnp.concatenate([part[:, i : i + span] for i in cuts], axis=2)
+            row = cuts.stop
 
 
 def all_from(own, axis, size):
@@ -102,15 +102,22 @@
     out[...] = hidden.reshape(out.shape)
 
 
-def down_kernel(first_ref, c_ref, *refs):
-    parts, (hidden, down, theirs, mine) = refs[:NY], refs[NY:]
+def product(core, hidden, down, out):
+    full = down[...].reshape(-1, down.shape[3])
+    act = hidden[:, core].reshape(-1, full.shape[1])
+    dims = (((1,), (1,)), ((), ()))
+    got = lax.dot_general(act, full, dims, preferred_element_type=jnp.float32)
+    out[...] = got.reshape(out.shape).astype(out.dtype)
+
+
+def theirs_kernel(first_ref, c_ref, *refs):
+    parts, (hidden, down, theirs) = refs[:NY], refs[NY:]
     put(first_ref, parts, (down,))
-    full = down[...].reshape(-1, down.shape[3])
-    dims = (((1,), (1,)), ((), ()))
-    for out, core in ((theirs, 1 - c_ref[0]), (mine, c_ref[0])):
-        act = hidden[:, core].reshape(-1, full.shape[1])
-        got = lax.dot_general(act, full, dims, preferred_element_type=jnp.float32)
-        out[...] = got.reshape(out.shape).astype(out.dtype)
+    product(1 - c_ref[0], hidden, down, theirs)
+
+
+def mine_kernel(c_ref, hidden, down, mine):
+    product(c_ref[0], hidden, down, mine)
 
 
 def on_core(kernel, scalars, arrays, outs, scratch=(), limit=None):
@@ -188,22 +195,27 @@
     )
 
     parts = all_from(first[:, 2 * one : cut], "y", NY)
-    down_serve, theirs, mine = on_core(
-        down_kernel,
+    hidden = held(hidden)
+    down_serve, theirs = on_core(
+        theirs_kernel,
         (first_block, c),
-        [held(a) for a in (*parts, hidden)],
-        [
-            placed,
-            pltpu.VMEM((NX, count // XC, width), bf16),
-            pltpu.VMEM((NX, count // XC, width), f32),
-        ],
+        (*[held(a) for a in parts], hidden),
+        [pltpu.VMEM(placed.shape, bf16), pltpu.VMEM((NX, count // XC, width), bf16)],
+        limit=16 << 20,
+    )
+    arrived = swap_core(theirs)
+    (mine,) = on_core(
+        mine_kernel,
+        (c,),
+        (hidden, held(down_serve)),
+        [pltpu.VMEM((NX, count // XC, width), f32)],
         limit=16 << 20,
     )
     gate_serve, up_serve, down_serve = (
         matrix.reshape(1, width, block) for matrix in (gate_serve, up_serve, down_serve)
     )
 
-    chip = (mine + swap_core(theirs).astype(jnp.float32)).astype(jnp.bfloat16)
+    chip = (mine + arrived.astype(jnp.float32)).astype(jnp.bfloat16)
     by_x = lax.all_to_all(chip, "x", 0, 0, tiled=True).astype(jnp.float32).sum(axis=0)
     by_x = by_x.astype(jnp.bfloat16).reshape(NZ, own_rows, width)
     by_z = lax.all_to_all(by_x, "z", 0, 0, tiled=True).astype(jnp.float32).sum(axis=0)

time: 176 us -> 176 us (level)
  blocking collectives: 94.6 us -> 74.8 us
  waiting for transfers between devices: 35.5 us -> 48 us
  starting transfers between devices: 33.2 us -> 39.2 us
    all_to_all x1 -> x0, blocking collectives: 19.7 us -> none  [per_device(): lax.all_to_all(by_x, 'z', 0, 0, tiled=True).astype(jnp.float32).sum(axis=0)]
    all_to_all x0 -> x1, waiting for transfers between devices: none -> 13 us  [per_device(): lax.all_to_all(by_x, 'z', 0, 0, tiled=True).astype(jnp.float32).sum(axis=0)]
    all_to_all x0 -> x1, starting transfers between devices: none -> 5.98 us  [per_device(): lax.all_to_all(by_x, 'z', 0, 0, tiled=True).astype(jnp.float32).sum(axis=0)]
    pallas_call x4 -> x5, Pallas kernels: 6.86 us -> 6.56 us  [on_core(): pl.pallas_call(kernel, out_shape=outs, in_specs=[smem] * len(scalars) + [...]
  transfers between devices with their start and end apart: 9 -> 10, of which waited for: 6 -> 7; matrix products, arithmetic and copies ran while one was open for 1% -> 2% of each run, Pallas kernels for 1% -> 1%
where the time goes in v3:
time: 176 us; the launch traced here: 175 us
  blocking collectives  74.8 us (42%)
  waiting for transfers between devices  48 us (27%)
  starting transfers between devices  39.2 us (22%)
  Pallas kernels  6.56 us (4%)
  local copies, waits for them, and re-layouts  4.2 us (2%)
    all_to_all x1, blocking collectives, per_device(): first = lax.all_to_all(sorted_by_z, 'z', 0, 0, tiled=True)  60.9 us
    ppermute x6, waiting for transfers between devices, shift(): lax.ppermute(array, axis, [(i, (i + by) % size) for i in range(size)])  22 us
    ppermute x6, starting transfers between devices, shift(): lax.ppermute(array, axis, [(i, (i + by) % size) for i in range(size)])  18.5 us
    all_to_all x1, blocking collectives, per_device(): lax.all_to_all(chip, 'x', 0, 0, tiled=True).astype(jnp.float32).sum(axis=0)  14 us
    all_to_all x1, waiting for transfers between devices, per_device(): lax.all_to_all(by_x, 'z', 0, 0, tiled=True).astype(jnp.float32).sum(axis=0)  13 us
    all_to_all x1, waiting for transfers between devices, per_device(): lax.all_to_all(local.reshape(XC * NY, 3, depth, block), ('x', 'c', 'y'),...  11.6 us
    all_to_all x1, starting transfers between devices, per_device(): lax.all_to_all(local.reshape(XC * NY, 3, depth, block), ('x', 'c', 'y'),...  9.28 us
    pallas_call x5, Pallas kernels, on_core(): pl.pallas_call(kernel, out_shape=outs, in_specs=[smem] * len(scalars) + [...  6.56 us
  transfers between devices with their start and end apart: 10, of which 7 were waited for; matrix products, arithmetic and copies ran while one was open for 2% of the time, Pallas kernels for 1%

profile of v3, /device:TPU:24, one launch (start us, length us, event | category | flops | bytes accessed | tf_op | source)
XLA Modules:
  0.0 175.3 jit_solution(12573947617953517231)
XLA Ops:
  0.6 2.4 %shard_map.102 = bf16[8,4,3,16,256]{4,3,2,1,0:T(8,128)(2,1)} custom-call(s32[1]{0:T(128)} %bitcast.3.x_ref, f32[1,16]{1,0:T(1,128)} %bitcast.17, f32[4,16,2048]{2,1,0:T(8,128)} %gate.1, f32[4,16,2048]{2,1,0:T(8,128)} %up.1, f32[4,16,2048]{2,1,0:T(8,128)} %down.1), custom_call_target="tpu_custom_call" | custom-call | tf_op jit(solution)/shard_map/pallas_call | solution.py:125
  3.0 0.0 copy-start.1
  3.0 0.0 copy-start.2
  3.0 0.0 copy-start.3
  3.0 9.3 %all-to-all-start = ((bf16[32,3,16,256]{3,2,1,0:T(8,128)(2,1)}), bf16[32,3,16,256]{3,2,1,0:T(8,128)(2,1)S(1)}, u32[]{:S(2)}, u32[]{:S(2)}) async-start(bf16[32,3,16,256]{3,2,1,0:T(8,128)(2,1)} %bitcast.5), calls=%async_computation | async-start | bytes 1572864 | tf_op jit(solution)/shard_map/all_to_all | solution.py:155
  12.3 0.0 copy-done.1
  12.3 0.1 convert_reduce_fusion
  12.5 0.2 fusion.3
  12.7 0.1 fusion.4
  12.8 0.0 copy-done.2
  12.8 0.2 slice_reduce_fusion.1
  13.0 0.0 copy-done.3
  13.0 0.2 fusion.8
  13.2 0.1 fusion.7
  13.3 11.6 %all-to-all-done = bf16[32,3,16,256]{3,2,1,0:T(8,128)(2,1)S(1)} async-done(((bf16[32,3,16,256]{3,2,1,0:T(8,128)(2,1)}), bf16[32,3,16,256]{3,2,1,0:T(8,128)(2,1)S(1)}, u32[]{:S(2)}, u32[]{:S(2)}) %all-to-all-start) | async-done | bytes 786464 | tf_op jit(solution)/shard_map/all_to_all | solution.py:155
  24.9 0.2 shard_map.103
  25.1 60.9 %all_to_all.25 = bf16[16,232,128]{2,1,0:T(8,128)(2,1)S(1)} all-to-all(bf16[16,232,128]{2,1,0:T(8,128)(2,1)S(1)} %shard_map.103), channel_id=1, replica_groups=mesh['z'=16,'x'=4,'c'=2,'y'=4] {'z'}, dimensions={0} | all-to-all | bytes 1900544 | tf_op jit(solution)/shard_map/all_to_all | solution.py:178
  85.9 0.0 copy-start
  86.0 0.1 reshape.73
  86.1 1.2 broadcast_in_dim.5
  87.2 3.6 %all-to-all-start.2 = ((bf16[8,32,2176]{2,1,0:T(8,128)(2,1)}), bf16[8,32,2176]{2,1,0:T(8,128)(2,1)S(1)}, u32[]{:S(2)}, u32[]{:S(2)}) async-start(bf16[8,32,2176]{2,1,0:T(8,128)(2,1)} %broadcast_in_dim.5), calls=%async_computation.2 | async-start | bytes 2228224 | tf_op jit(solution)/shard_map/all_to_all | solution.py:185
  90.8 0.0 copy-done
  90.9 3.4 %collective-permute-start = (bf16[16,128,128]{2,1,0:T(8,128)(2,1)S(1)}, bf16[16,128,128]{2,1,0:T(8,128)(2,1)S(1)}, u32[]{:S(2)}, u32[]{:S(2)}) collective-permute-start(bf16[16,128,128]{2,1,0:T(8,128)(2,1)S(1)} %slice.34.refs_0_), channel_id=1, source_target_pairs={{0,1},{1,2},{2,3},{3,0},{4,5},{5,6},{6,7},{7,4},{8,9},{9,10},{10,1... | collective-permute-start | bytes 1572872 | tf_op jit(solution)/shard_map/ppermute | solution.py:36
  94.3 3.0 %collective-permute-start.1 = (bf16[16,128,128]{2,1,0:T(8,128)(2,1)S(1)}, bf16[16,128,128]{2,1,0:T(8,128)(2,1)S(1)}, u32[]{:S(2)}, u32[]{:S(2)}) collective-permute-start(bf16[16,128,128]{2,1,0:T(8,128)(2,1)S(1)} %slice.34.refs_0_), channel_id=1, source_target_pairs={{0,2},{1,3},{2,0},{3,1},{4,6},{5,7},{6,4},{7,5},{8,10},{9,11},{10,... | collective-permute-start | bytes 1572872 | tf_op jit(solution)/shard_map/ppermute | solution.py:36
  97.2 2.8 %collective-permute-start.2 = (bf16[16,128,128]{2,1,0:T(8,128)(2,1)S(1)}, bf16[16,128,128]{2,1,0:T(8,128)(2,1)S(1)}, u32[]{:S(2)}, u32[]{:S(2)}) collective-permute-start(bf16[16,128,128]{2,1,0:T(8,128)(2,1)S(1)} %slice.34.refs_0_), channel_id=1, source_target_pairs={{0,3},{1,0},{2,1},{3,2},{4,7},{5,4},{6,5},{7,6},{8,11},{9,8},{10,9... | collective-permute-start | bytes 1572872 | tf_op jit(solution)/shard_map/ppermute | solution.py:36
  100.1 1.0 slice.37.refs_0_
  101.1 4.2 %collective-permute-start.3 = (bf16[16,64,128]{2,1,0:T(8,128)(2,1)S(1)}, bf16[16,64,128]{2,1,0:T(8,128)(2,1)}, u32[]{:S(2)}, u32[]{:S(2)}) collective-permute-start(bf16[16,64,128]{2,1,0:T(8,128)(2,1)S(1)} %slice.37.refs_0_), channel_id=1, source_target_pairs={{0,1},{1,2},{2,3},{3,0},{4,5},{5,6},{6,7},{7,4},{8,9},{9,10},{10,1... | collective-permute-start | bytes 786440 | tf_op jit(solution)/shard_map/ppermute | solution.py:36
  105.3 3.2 %collective-permute-start.4 = (bf16[16,64,128]{2,1,0:T(8,128)(2,1)S(1)}, bf16[16,64,128]{2,1,0:T(8,128)(2,1)}, u32[]{:S(2)}, u32[]{:S(2)}) collective-permute-start(bf16[16,64,128]{2,1,0:T(8,128)(2,1)S(1)} %slice.37.refs_0_), channel_id=1, source_target_pairs={{0,2},{1,3},{2,0},{3,1},{4,6},{5,7},{6,4},{7,5},{8,10},{9,11},{10,... | collective-permute-start | bytes 786440 | tf_op jit(solution)/shard_map/ppermute | solution.py:36
  108.5 8.8 %collective-permute-done.refs_1_ = bf16[16,128,128]{2,1,0:T(8,128)(2,1)S(1)} collective-permute-done((bf16[16,128,128]{2,1,0:T(8,128)(2,1)S(1)}, bf16[16,128,128]{2,1,0:T(8,128)(2,1)S(1)}, u32[]{:S(2)}, u32[]{:S(2)}) %collective-permute-start) | collective-permute-done | bytes 524320 | tf_op jit(solution)/shard_map/ppermute | solution.py:36
  117.2 1.9 %collective-permute-start.5 = (bf16[16,64,128]{2,1,0:T(8,128)(2,1)S(1)}, bf16[16,64,128]{2,1,0:T(8,128)(2,1)}, u32[]{:S(2)}, u32[]{:S(2)}) collective-permute-start(bf16[16,64,128]{2,1,0:T(8,128)(2,1)S(1)} %slice.37.refs_0_), channel_id=1, source_target_pairs={{0,3},{1,0},{2,1},{3,2},{4,7},{5,4},{6,5},{7,6},{8,11},{9,8},{10,9... | collective-permute-start | bytes 786440 | tf_op jit(solution)/shard_map/ppermute | solution.py:36
  119.2 0.0 collective-permute-done.1.refs_2_
  119.2 4.6 %collective-permute-done.2.refs_3_ = bf16[16,128,128]{2,1,0:T(8,128)(2,1)S(1)} collective-permute-done((bf16[16,128,128]{2,1,0:T(8,128)(2,1)S(1)}, bf16[16,128,128]{2,1,0:T(8,128)(2,1)S(1)}, u32[]{:S(2)}, u32[]{:S(2)}) %collective-permute-start.2) | collective-permute-done | bytes 524320 | tf_op jit(solution)/shard_map/ppermute | solution.py:36
  123.8 0.0 all-to-all-done.2
  123.8 1.9 %shard_map.104 = (bf16[16,4,32,256]{3,2,1,0:T(8,128)(2,1)}, bf16[16,4,32,256]{3,2,1,0:T(8,128)(2,1)}, bf16[4,2,32,256]{3,2,1,0:T(8,128)(2,1)S(1)}) custom-call(s32[1]{0:T(128)} %bitcast.first_ref, s32[1]{0:T(128)} %bitcast.1.expert_ref, bf16[16,128,128]{2,1,0:T(8,128)(2,1)S(1)} %slice.34.refs_0_, bf16[16,128,128]{2,1,0:T(8,128)(2,1)S(1)} %collective-permute-done.refs_1_, ...), custom_call_target="tpu_custom_call" | custom-call | tf_op jit(solution)/shard_map/pallas_call | solution.py:125
  125.7 0.0 collective-permute-done.3.refs_1_
  125.7 3.8 %collective-permute-done.4.refs_2_ = bf16[16,64,128]{2,1,0:T(8,128)(2,1)} collective-permute-done((bf16[16,64,128]{2,1,0:T(8,128)(2,1)S(1)}, bf16[16,64,128]{2,1,0:T(8,128)(2,1)}, u32[]{:S(2)}, u32[]{:S(2)}) %collective-permute-start.4) | collective-permute-done | bytes 262176 | tf_op jit(solution)/shard_map/ppermute | solution.py:36
  129.5 4.8 %collective-permute-done.5.refs_3_ = bf16[16,64,128]{2,1,0:T(8,128)(2,1)} collective-permute-done((bf16[16,64,128]{2,1,0:T(8,128)(2,1)S(1)}, bf16[16,64,128]{2,1,0:T(8,128)(2,1)}, u32[]{:S(2)}, u32[]{:S(2)}) %collective-permute-start.5) | collective-permute-done | bytes 262176 | tf_op jit(solution)/shard_map/ppermute | solution.py:36
  134.3 1.7 shard_map.105
  136.0 1.9 %collective-permute-start.6 = (bf16[4,32,2048]{2,1,0:T(8,128)(2,1)S(1)}, bf16[4,32,2048]{2,1,0:T(8,128)(2,1)S(1)}, u32[]{:S(2)}, u32[]{:S(2)}) collective-permute-start(bf16[4,32,2048]{2,1,0:T(8,128)(2,1)S(1)} %get-tuple-element.13), channel_id=1, source_target_pairs={{0,4},{4,0},{1,5},{5,1},{2,6},{6,2},{3,7},{7,3},{8,12},{12,8},{9,1... | collective-permute-start | bytes 1572872 | tf_op jit(solution)/shard_map/ppermute | solution.py:40
  137.9 0.5 shard_map.106
  138.4 1.4 collective-permute-done.6
  139.8 0.1 add_convert_fusion
  139.9 14.0 %all_to_all.26 = bf16[4,32,2048]{2,1,0:T(8,128)(2,1)S(1)} all-to-all(bf16[4,32,2048]{2,1,0:T(8,128)(2,1)S(1)} %add_convert_fusion), channel_id=1, replica_groups=mesh['z'=16,'x'=4,'c'=2,'y'=4] {'x'}, dimensions={0} | all-to-all | bytes 1048576 | tf_op jit(solution)/shard_map/all_to_all | solution.py:219
  153.9 0.1 reduce_sum.44
  154.0 0.7 reshape.80
  154.7 6.0 %all-to-all-start.4 = ((bf16[16,2,2048]{2,1,0:T(2,128)(2,1)}), bf16[16,2,2048]{2,1,0:T(2,128)(2,1)S(1)}, u32[]{:S(2)}, u32[]{:S(2)}) async-start(bf16[16,2,2048]{2,1,0:T(2,128)(2,1)} %reshape.80), calls=%async_computation.4 | async-start | bytes 262144 | tf_op jit(solution)/shard_map/all_to_all | solution.py:221
  160.7 1.0 copy.13
  161.7 13.0 %all-to-all-done.4 = bf16[16,2,2048]{2,1,0:T(2,128)(2,1)S(1)} async-done(((bf16[16,2,2048]{2,1,0:T(2,128)(2,1)}), bf16[16,2,2048]{2,1,0:T(2,128)(2,1)S(1)}, u32[]{:S(2)}, u32[]{:S(2)}) %all-to-all-start.4) | async-done | bytes 131104 | tf_op jit(solution)/shard_map/all_to_all | solution.py:221
  174.6 0.7 reduce_sum.45
  (8 shorter events, 0.1 us)
Async XLA Ops:
  3.0 9.3 %copy-start.1 = (bf16[2,2048]{1,0:T(2,128)(2,1)S(1)}, bf16[2,2048]{1,0:T(2,128)(2,1)}, u32[]{:S(2)}) copy-start(bf16[2,2048]{1,0:T(2,128)(2,1)} %param.7) | copy-start | bytes 24580
  3.0 9.8 %copy-start.2 = (s32[2,2]{1,0:T(2,128)S(1)}, s32[2,2]{1,0:T(2,128)}, u32[]{:S(2)}) copy-start(s32[2,2]{1,0:T(2,128)} %param.8) | copy-start | bytes 52
  3.0 9.9 %copy-start.3 = (f32[2,2]{1,0:T(2,128)S(1)}, f32[2,2]{1,0:T(2,128)}, u32[]{:S(2)}) copy-start(f32[2,2]{1,0:T(2,128)} %param.9) | copy-start | bytes 52
  3.0 21.9 %all-to-all-start = ((bf16[32,3,16,256]{3,2,1,0:T(8,128)(2,1)}), bf16[32,3,16,256]{3,2,1,0:T(8,128)(2,1)S(1)}, u32[]{:S(2)}, u32[]{:S(2)}) async-start(bf16[32,3,16,256]{3,2,1,0:T(8,128)(2,1)} %bitcast.5), calls=%async_computation | async-start | bytes 1572864 | tf_op jit(solution)/shard_map/all_to_all | solution.py:155
  85.9 4.9 %copy-start = (bf16[16,232,128]{2,1,0:T(8,128)(2,1)}, bf16[16,232,128]{2,1,0:T(8,128)(2,1)S(1)}, u32[]{:S(2)}) copy-start(bf16[16,232,128]{2,1,0:T(8,128)(2,1)S(1)} %all_to_all.25) | copy-start | bytes 2850820
  87.2 36.6 %all-to-all-start.2 = ((bf16[8,32,2176]{2,1,0:T(8,128)(2,1)}), bf16[8,32,2176]{2,1,0:T(8,128)(2,1)S(1)}, u32[]{:S(2)}, u32[]{:S(2)}) async-start(bf16[8,32,2176]{2,1,0:T(8,128)(2,1)} %broadcast_in_dim.5), calls=%async_computation.2 | async-start | bytes 2228224 | tf_op jit(solution)/shard_map/all_to_all | solution.py:185
  90.9 26.4 %collective-permute-start = (bf16[16,128,128]{2,1,0:T(8,128)(2,1)S(1)}, bf16[16,128,128]{2,1,0:T(8,128)(2,1)S(1)}, u32[]{:S(2)}, u32[]{:S(2)}) collective-permute-start(bf16[16,128,128]{2,1,0:T(8,128)(2,1)S(1)} %slice.34.refs_0_), channel_id=1, source_target_pairs={{0,1},{1,2},{2,3},{3,0},{4,5},{5,6},{6,7},{7,4},{8,9},{9,10},{10,1... | collective-permute-start | bytes 1572872 | tf_op jit(solution)/shard_map/ppermute | solution.py:36
  94.3 24.9 %collective-permute-start.1 = (bf16[16,128,128]{2,1,0:T(8,128)(2,1)S(1)}, bf16[16,128,128]{2,1,0:T(8,128)(2,1)S(1)}, u32[]{:S(2)}, u32[]{:S(2)}) collective-permute-start(bf16[16,128,128]{2,1,0:T(8,128)(2,1)S(1)} %slice.34.refs_0_), channel_id=1, source_target_pairs={{0,2},{1,3},{2,0},{3,1},{4,6},{5,7},{6,4},{7,5},{8,10},{9,11},{10,... | collective-permute-start | bytes 1572872 | tf_op jit(solution)/shard_map/ppermute | solution.py:36
  97.2 26.6 %collective-permute-start.2 = (bf16[16,128,128]{2,1,0:T(8,128)(2,1)S(1)}, bf16[16,128,128]{2,1,0:T(8,128)(2,1)S(1)}, u32[]{:S(2)}, u32[]{:S(2)}) collective-permute-start(bf16[16,128,128]{2,1,0:T(8,128)(2,1)S(1)} %slice.34.refs_0_), channel_id=1, source_target_pairs={{0,3},{1,0},{2,1},{3,2},{4,7},{5,4},{6,5},{7,6},{8,11},{9,8},{10,9... | collective-permute-start | bytes 1572872 | tf_op jit(solution)/shard_map/ppermute | solution.py:36
  101.1 24.6 %collective-permute-start.3 = (bf16[16,64,128]{2,1,0:T(8,128)(2,1)S(1)}, bf16[16,64,128]{2,1,0:T(8,128)(2,1)}, u32[]{:S(2)}, u32[]{:S(2)}) collective-permute-start(bf16[16,64,128]{2,1,0:T(8,128)(2,1)S(1)} %slice.37.refs_0_), channel_id=1, source_target_pairs={{0,1},{1,2},{2,3},{3,0},{4,5},{5,6},{6,7},{7,4},{8,9},{9,10},{10,1... | collective-permute-start | bytes 786440 | tf_op jit(solution)/shard_map/ppermute | solution.py:36
  105.3 24.2 %collective-permute-start.4 = (bf16[16,64,128]{2,1,0:T(8,128)(2,1)S(1)}, bf16[16,64,128]{2,1,0:T(8,128)(2,1)}, u32[]{:S(2)}, u32[]{:S(2)}) collective-permute-start(bf16[16,64,128]{2,1,0:T(8,128)(2,1)S(1)} %slice.37.refs_0_), channel_id=1, source_target_pairs={{0,2},{1,3},{2,0},{3,1},{4,6},{5,7},{6,4},{7,5},{8,10},{9,11},{10,... | collective-permute-start | bytes 786440 | tf_op jit(solution)/shard_map/ppermute | solution.py:36
  117.2 17.0 %collective-permute-start.5 = (bf16[16,64,128]{2,1,0:T(8,128)(2,1)S(1)}, bf16[16,64,128]{2,1,0:T(8,128)(2,1)}, u32[]{:S(2)}, u32[]{:S(2)}) collective-permute-start(bf16[16,64,128]{2,1,0:T(8,128)(2,1)S(1)} %slice.37.refs_0_), channel_id=1, source_target_pairs={{0,3},{1,0},{2,1},{3,2},{4,7},{5,4},{6,5},{7,6},{8,11},{9,8},{10,9... | collective-permute-start | bytes 786440 | tf_op jit(solution)/shard_map/ppermute | solution.py:36
  136.0 3.8 %collective-permute-start.6 = (bf16[4,32,2048]{2,1,0:T(8,128)(2,1)S(1)}, bf16[4,32,2048]{2,1,0:T(8,128)(2,1)S(1)}, u32[]{:S(2)}, u32[]{:S(2)}) collective-permute-start(bf16[4,32,2048]{2,1,0:T(8,128)(2,1)S(1)} %get-tuple-element.13), channel_id=1, source_target_pairs={{0,4},{4,0},{1,5},{5,1},{2,6},{6,2},{3,7},{7,3},{8,12},{12,8},{9,1... | collective-permute-start | bytes 1572872 | tf_op jit(solution)/shard_map/ppermute | solution.py:40
  154.7 19.9 %all-to-all-start.4 = ((bf16[16,2,2048]{2,1,0:T(2,128)(2,1)}), bf16[16,2,2048]{2,1,0:T(2,128)(2,1)S(1)}, u32[]{:S(2)}, u32[]{:S(2)}) async-start(bf16[16,2,2048]{2,1,0:T(2,128)(2,1)} %reshape.80), calls=%async_computation.4 | async-start | bytes 262144 | tf_op jit(solution)/shard_map/all_to_all | solution.py:221
